TPU v7x, 32 devices: a whole 2x2x4 slice. The times are simulated.
32 devices in a mesh: st: 8 (over z, x), tp: 4 (over y, core).
Axes of the slice: x: 2, y: 2, z: 4, core: 2. Of those that a mesh axis runs over, the one named last changes fastest.
Arguments:
- symbol_activations: bfloat16 [6144, 2048], P('st', 'tp'), may hold values from -6 to 6
- document_corpus: bfloat16 [128, 96, 2048], P('st'), may hold values from -6 to 6
- document_choice_matrix: int32 [48, 4], P('st'), may hold values from 0 to 127, as said below
- memory_probe_matrix: bfloat16 [2048, 1024], P(None, 'tp'), may hold values from -0.125 to 0.125
- memory_lookup_matrix: bfloat16 [2048, 1024], P(None, 'tp'), may hold values from -0.125 to 0.125
- memory_content_matrix: bfloat16 [2048, 1024], P(None, 'tp'), may hold values from -0.125 to 0.125
- valve_matrix: bfloat16 [2048, 16], replicated, may hold values from -0.125 to 0.125
- valve_biases: float32 [16], replicated, may hold values from -3 to 9
- added_decay_logit: float32 [6144, 8], P('st'), may hold values from -1 to 0
- facet_rescale_factor: float32 [1024], P('tp'), may hold values from 0.1 to 1.9
- document_probe_matrix: bfloat16 [2048, 1024], P(None, 'tp'), may hold values from -0.125 to 0.125
- document_lookup_matrix: bfloat16 [2048, 1024], P(None, 'tp'), may hold values from -0.125 to 0.125
- document_content_matrix: bfloat16 [2048, 1024], P(None, 'tp'), may hold values from -0.125 to 0.125
- document_rescale_factor: float32 [2048], replicated, may hold values from 0.1 to 1.9
- affinity_scaling: float32 [8], replicated, may hold values from 8 to 1200
- fetched_mixer_matrix: bfloat16 [2048, 1024], P(None, 'tp'), may hold values from -0.125 to 0.125
Outputs:
- mixed: bfloat16 [6144, 1024], P('st', 'tp')
Inputs may be any that keep to these rules, and one draw needn't show every extreme that they name: `document_choice_matrix`: row b names the 4 passages that block b reads; passage p is held by index p // 16 of st. Among the rows of one sequence at most 6 ids name passages of one holder, and some holder is named exactly 6 times by each sequence.
All inputs are finite; a program needn't handle non-finite values.
Results may differ from a plain program's by a relative error of at most 0.0095.
The roundings to bfloat16 on the way count: a program that leaves them out, or rounds other values in their place, can miss the bound.
Values may be sent and summed in bfloat16 or wider, within the bound.
A program may use at most 128 MiB of HBM per device.

v0:
```python
import jax
import jax.numpy as jnp
from jax import lax
from jax.sharding import PartitionSpec as P

FACET_COUNT = 8
LANE_DIMENSION = 128
SEG = 128


EPSILON = 1e-06
EMPTY_LOG = -1e30
HIGHEST = lax.Precision.HIGHEST


def rms_scale(tensor):
    return lax.rsqrt(jnp.mean(tensor * tensor, axis=-1, keepdims=True) + EPSILON)


def cell_blocks(queries, key_rows, value_rows, input_logits, forget_log_gate):
    head_count, length, facet_dimension = queries.shape
    block_count = length // SEG

    def to_blocks(tensor):
        shaped = tensor.reshape((head_count, block_count, SEG) + tensor.shape[2:])
        return jnp.moveaxis(shaped, 1, 0)

    causal = jnp.tril(jnp.ones((SEG, SEG), dtype=bool))

    def advance(carry, blocks):
        memory, normal, stabilizer = carry
        query_part, key_part, value_part, input_part, forget_part = blocks
        cumulative = jnp.cumsum(forget_part, axis=-1)
        log_weight = jnp.where(
            causal,
            cumulative[:, :, None] - cumulative[:, None, :] + input_part[:, None, :],
            -jnp.inf,
        )
        carried = cumulative + stabilizer[:, None]
        peak = jnp.maximum(carried, jnp.max(log_weight, axis=-1))
        weight = jnp.exp(log_weight - peak[:, :, None])
        old_weight = jnp.exp(carried - peak)
        affinity_logits = (
            jnp.einsum("htd,hsd->hts", query_part, key_part, precision=HIGHEST) * weight
        )
        numerator = old_weight[:, :, None] * jnp.einsum(
            "htd,hde->hte", query_part, memory, precision=HIGHEST
        ) + jnp.einsum("hts,hse->hte", affinity_logits, value_part, precision=HIGHEST)
        denominator = old_weight * jnp.einsum(
            "htd,hd->ht", query_part, normal, precision=HIGHEST
        ) + jnp.sum(affinity_logits, axis=-1)
        final_output = numerator / jnp.maximum(jnp.abs(denominator), jnp.exp(-peak))[:, :, None]
        last_weight = weight[:, -1, :]
        old_last = old_weight[:, -1]
        weighted_keys = last_weight[:, :, None] * key_part
        memory = old_last[:, None, None] * memory + jnp.einsum(
            "hsd,hse->hde", weighted_keys, value_part, precision=HIGHEST
        )
        normal = old_last[:, None] * normal + jnp.sum(weighted_keys, axis=1)
        return ((memory, normal, peak[:, -1]), final_output)

    initial = (
        jnp.zeros((head_count, facet_dimension, facet_dimension), jnp.float32),
        jnp.zeros((head_count, facet_dimension), jnp.float32),
        jnp.full((head_count,), EMPTY_LOG, jnp.float32),
    )
    scaled_keys = key_rows * facet_dimension ** (-0.5)
    final_state, outcome = lax.scan(
        advance,
        initial,
        (
            to_blocks(queries),
            to_blocks(scaled_keys),
            to_blocks(value_rows),
            to_blocks(input_logits),
            to_blocks(forget_log_gate),
        ),
    )
    return jnp.moveaxis(outcome, 0, 1).reshape(head_count, length, facet_dimension)


def document_lookup_update(probe_vectors, segment_lookups, segment_contents, facet_scales):
    facet_dimension = probe_vectors.shape[-1]
    affinity_logits = jnp.einsum(
        "bqhd,bkhd->bhqk", probe_vectors, segment_lookups, preferred_element_type=jnp.float32
    )
    ask_scale = rms_scale(probe_vectors.astype(jnp.float32))[..., 0]
    key_scale = rms_scale(segment_lookups.astype(jnp.float32))[..., 0]
    affinity_logits = affinity_logits * jnp.transpose(ask_scale, (0, 2, 1))[:, :, :, None]
    affinity_logits = affinity_logits * jnp.transpose(key_scale, (0, 2, 1))[:, :, None, :]
    affinity_logits = affinity_logits * (facet_scales / facet_dimension)[None, :, None, None]
    peak = jnp.max(affinity_logits, axis=-1, keepdims=True)
    exp_scores = jnp.exp(affinity_logits - peak)
    weights = (exp_scores / jnp.sum(exp_scores, axis=-1, keepdims=True)).astype(jnp.bfloat16)
    return jnp.einsum(
        "bhqk,bkhd->bqhd", weights, segment_contents, preferred_element_type=jnp.float32
    )


def project_rows(
    passage_rows, document_rescale_factor, document_lookup_matrix, document_content_matrix
):
    widened = passage_rows.reshape(-1, passage_rows.shape[-1]).astype(jnp.float32)
    normed = (widened * rms_scale(widened) * document_rescale_factor).astype(jnp.bfloat16)
    out_shape = passage_rows.shape[:-1] + (document_lookup_matrix.shape[1],)
    key_part = jnp.dot(normed, document_lookup_matrix, preferred_element_type=jnp.float32).astype(
        jnp.bfloat16
    )
    value_part = jnp.dot(
        normed, document_content_matrix, preferred_element_type=jnp.float32
    ).astype(jnp.bfloat16)
    return (key_part.reshape(out_shape), value_part.reshape(out_shape))


def local(
    symbol_activations,
    document_corpus,
    document_choice_matrix,
    memory_probe_matrix,
    memory_lookup_matrix,
    memory_content_matrix,
    valve_matrix,
    valve_biases,
    added_decay_logit,
    facet_rescale_factor,
    document_probe_matrix,
    document_lookup_matrix,
    document_content_matrix,
    document_rescale_factor,
    affinity_scaling,
    fetched_mixer_matrix,
):
    head_index = lax.axis_index("tp")
    local_width = memory_probe_matrix.shape[1]
    local_facets = local_width // LANE_DIMENSION
    tok_rows = symbol_activations.shape[0]
    joined = jnp.concatenate(
        [
            memory_probe_matrix,
            memory_lookup_matrix,
            memory_content_matrix,
            document_probe_matrix,
            fetched_mixer_matrix,
        ],
        axis=1,
    )
    token_piece = lax.all_gather(symbol_activations, "tp", axis=1, tiled=True)
    projected = jnp.dot(token_piece, joined, preferred_element_type=jnp.float32)
    gate_preactivation = jnp.dot(token_piece, valve_matrix, preferred_element_type=jnp.float32)
    queries = projected[:, :local_width].astype(jnp.bfloat16)
    key_rows = projected[:, local_width : 2 * local_width].astype(jnp.bfloat16)
    value_rows = projected[:, 2 * local_width : 3 * local_width].astype(jnp.bfloat16)
    probe_vectors = projected[:, 3 * local_width : 4 * local_width].astype(jnp.bfloat16)
    mix_logits = projected[:, 4 * local_width :]
    first_facet = head_index * local_facets
    gate_preactivation = gate_preactivation + valve_biases
    input_logits = lax.dynamic_slice_in_dim(gate_preactivation, first_facet, local_facets, 1)
    forget_logits = lax.dynamic_slice_in_dim(
        gate_preactivation, FACET_COUNT + first_facet, local_facets, 1
    )
    forget_log_gate = jax.nn.log_sigmoid(forget_logits) + lax.dynamic_slice_in_dim(
        added_decay_logit, first_facet, local_facets, 1
    )

    def heads_first(tensor):
        return jnp.transpose(
            tensor.astype(jnp.float32).reshape(tok_rows, local_facets, LANE_DIMENSION), (1, 0, 2)
        )

    cell_out = cell_blocks(
        heads_first(queries),
        heads_first(key_rows),
        heads_first(value_rows),
        input_logits.T,
        forget_log_gate.T,
    )
    cell_out = (
        cell_out
        * rms_scale(cell_out)
        * facet_rescale_factor.reshape(local_facets, 1, LANE_DIMENSION)
    )
    cell_out = jnp.transpose(cell_out, (1, 0, 2)).reshape(tok_rows, local_width)
    st_devices = lax.axis_size("st")
    flat_ids = document_choice_matrix.reshape(-1)
    request_count = flat_ids.shape[0]
    block_count = document_choice_matrix.shape[0]
    slot_cap = max(2, 2 * request_count // st_devices)
    per_owner = document_corpus.shape[0]
    owners = flat_ids // per_owner
    within = flat_ids % per_owner
    order_index = jnp.arange(request_count, dtype=jnp.int32)
    same_owner = (owners[:, None] == owners[None, :]) & (
        order_index[:, None] > order_index[None, :]
    )
    rank_among = jnp.sum(same_owner.astype(jnp.int32), axis=1)
    slot_index = owners * slot_cap + rank_among
    slot_hits = (
        slot_index[:, None] == jnp.arange(st_devices * slot_cap, dtype=jnp.int32)[None, :]
    ).astype(jnp.int32)
    outgoing = jnp.sum(slot_hits * within[:, None], axis=0).reshape(st_devices, slot_cap)
    incoming = lax.all_to_all(outgoing, "st", split_axis=0, concat_axis=0, tiled=True)
    shard_keys, shard_values = project_rows(
        document_corpus, document_rescale_factor, document_lookup_matrix, document_content_matrix
    )
    passage_keys, passage_values = (
        lax.all_to_all(shard_keys[incoming], "st", split_axis=0, concat_axis=0, tiled=True),
        lax.all_to_all(shard_values[incoming], "st", split_axis=0, concat_axis=0, tiled=True),
    )
    slot_keys = passage_keys.reshape(st_devices * slot_cap, -1, local_width)
    slot_values = passage_values.reshape(st_devices * slot_cap, -1, local_width)
    segment_lookups = slot_keys[slot_index].reshape(block_count, -1, local_facets, LANE_DIMENSION)
    segment_contents = slot_values[slot_index].reshape(
        block_count, -1, local_facets, LANE_DIMENSION
    )
    segment_probes = probe_vectors.reshape(block_count, -1, local_facets, LANE_DIMENSION)
    facet_scales = lax.dynamic_slice_in_dim(affinity_scaling, first_facet, local_facets, 0)
    fetched_result = document_lookup_update(
        segment_probes, segment_lookups, segment_contents, facet_scales
    ).reshape(tok_rows, local_width)
    return (cell_out + jax.nn.sigmoid(mix_logits) * fetched_result).astype(jnp.bfloat16)


def solution(mesh):
    return jax.shard_map(
        local,
        mesh=mesh,
        in_specs=(
            P("st", "tp"),
            P("st", None, None),
            P("st", None),
            P(None, "tp"),
            P(None, "tp"),
            P(None, "tp"),
            P(),
            P(),
            P("st", None),
            P("tp"),
            P(None, "tp"),
            P(None, "tp"),
            P(None, "tp"),
            P(),
            P(),
            P(None, "tp"),
        ),
        out_specs=P("st", "tp"),
        check_vma=False,
    )
```

profile of v0, /device:TPU:0, one launch (start us, length us, event | category | flops | bytes accessed | tf_op | source)
XLA Modules:
  0.0 228.0 jit_solution(18359715338860256959)
XLA Ops:
  8.5 7.3 %all-to-all-start = ((s32[8,1,6]{2,1,0:T(1,128)}), s32[8,1,6]{2,1,0:T(1,128)S(1)}, u32[]{:S(2)}, u32[]{:S(2)}) async-start(s32[8,1,6]{2,1,0:T(1,128)} %bitcast.24), calls=%async_computation | async-start | bytes 8192 | tf_op jit(solution)/shard_map/all_to_all | solution.py:201
  15.7 4.1 %multiply_reduce_fusion = f32[16,96]{1,0:T(8,128)S(1)} fusion(bf16[16,96,2048]{2,1,0:T(8,128)(2,1)} %param.19), kind=kLoop, calls=%fused_computation.56 | loop fusion | flops 9435648 | bytes 6297600 | tf_op jit(solution)/shard_map/reduce_sum | solution.py:17
  19.9 4.3 %fusion.33 = bf16[1536,2048]{1,0:T(8,128)(2,1)S(1)} fusion(f32[2048]{0:T(1024)S(1)} %copy-done.10, f32[1536]{0:T(1024)S(1)} %rsqrt.45, bf16[16,96,2048]{2,1,0:T(8,128)(2,1)} %param.19), kind=kLoop, calls=%fused_computation.55 | loop fusion | flops 12582912 | bytes 12597248 | tf_op jit(solution)/shard_map/convert_element_type | solution.py:104
  24.2 2.7 %copy-done.3 = bf16[1536,2048]{1,0:T(8,128)(2,1)} copy-done((bf16[1536,2048]{1,0:T(8,128)(2,1)}, bf16[1536,2048]{1,0:T(8,128)(2,1)S(1)}, u32[]{:S(2)}) %copy-start.3) | copy-done | bytes 6291480
  26.9 1.9 convolution_convert_fusion
  29.0 2.2 gather_fusion.2
  31.2 6.0 %all-to-all-start.2 = ((bf16[8,6,96,256]{3,2,1,0:T(8,128)(2,1)}), bf16[8,6,96,256]{3,2,1,0:T(8,128)(2,1)S(1)}, u32[]{:S(2)}, u32[]{:S(2)}) async-start(bf16[8,6,96,256]{3,2,1,0:T(8,128)(2,1)} %bitcast.31), calls=%async_computation.2 | async-start | bytes 4718592 | tf_op jit(solution)/shard_map/all_to_all | solution.py:206
  38.0 4.8 %convolution_convert_fusion.1 = bf16[1536,256]{1,0:T(8,128)(2,1)S(1)} fusion(bf16[1536,2048]{1,0:T(8,128)(2,1)} %copy-done.3, bf16[2048,256]{1,0:T(8,128)(2,1)} %param.30), kind=kOutput, calls=%fused_computation.59 | convolution fusion | flops 1611005952 | bytes 8126464 | tf_op jit(solution)/shard_map/dot_general | solution.py:109
  42.8 2.2 gather_fusion
  45.1 45.5 %all-to-all-done.2 = bf16[8,6,96,256]{3,2,1,0:T(8,128)(2,1)S(1)} async-done(((bf16[8,6,96,256]{3,2,1,0:T(8,128)(2,1)}), bf16[8,6,96,256]{3,2,1,0:T(8,128)(2,1)S(1)}, u32[]{:S(2)}, u32[]{:S(2)}) %all-to-all-start.2) | async-done | bytes 2359328 | tf_op jit(solution)/shard_map/all_to_all | solution.py:206
  90.5 4.7 %all-to-all-start.1 = ((bf16[8,6,96,256]{3,2,1,0:T(8,128)(2,1)}), bf16[8,6,96,256]{3,2,1,0:T(8,128)(2,1)}, u32[]{:S(2)}, u32[]{:S(2)}) async-start(bf16[8,6,96,256]{3,2,1,0:T(8,128)(2,1)} %bitcast.26), calls=%async_computation.1 | async-start | bytes 4718592 | tf_op jit(solution)/shard_map/all_to_all | solution.py:207
  95.4 1.3 constant_dynamic-update-slice_fusion.4
  96.8 1.4 constant_dynamic-update-slice_fusion.3
  98.2 1.4 constant_dynamic-update-slice_fusion.2
  99.8 2.3 %copy-done.8 = bf16[2048,1280]{1,0:T(8,128)(2,1)} copy-done((bf16[2048,1280]{1,0:T(8,128)(2,1)}, bf16[2048,1280]{1,0:T(8,128)(2,1)S(1)}, u32[]{:S(2)}) %copy-start.8) | copy-done | bytes 5242904
  102.1 1.8 gather_fusion.3
  103.9 2.8 %reshape.370 = bf16[6,384,2,128]{3,2,1,0:T(2,128)(2,1)S(1)} reshape(bf16[24,96,256]{2,1,0:T(8,128)(2,1)} %gather_fusion.3) | data formatting | bytes 2359296 | tf_op jit(solution)/shard_map/reshape | solution.py:211
  106.6 2.5 %multiply_reduce_fusion.1 = f32[6,384,2]{2,1,0:T(8,128)S(1)} fusion(bf16[6,384,2,128]{3,2,1,0:T(2,128)(2,1)S(1)} %reshape.370), kind=kLoop, calls=%fused_computation.63 | loop fusion | flops 1764864 | bytes 1198080 | tf_op jit(solution)/shard_map/reduce_sum | solution.py:17
  109.7 38.9 %all-to-all-done.1 = bf16[8,6,96,256]{3,2,1,0:T(8,128)(2,1)} async-done(((bf16[8,6,96,256]{3,2,1,0:T(8,128)(2,1)}), bf16[8,6,96,256]{3,2,1,0:T(8,128)(2,1)}, u32[]{:S(2)}, u32[]{:S(2)}) %all-to-all-start.1) | async-done | bytes 2359328 | tf_op jit(solution)/shard_map/all_to_all | solution.py:207
  148.6 2.3 %gather_fusion.1 = bf16[24,96,256]{2,1,0:T(8,128)(2,1)S(1)} fusion(bf16[48,96,256]{2,1,0:T(8,128)(2,1)} %bitcast.27, s32[1024]{0:T(1024)S(1)} %pad_clamp_fusion), kind=kCustom, calls=%fused_computation.1 | custom fusion | bytes 2359392 | tf_op jit(solution)/shard_map/gather | solution.py:212
  150.9 1.3 reshape.366
  152.1 9.7 %fusion.68 = (bf16[768,1280]{0,1:T(8,128)(2,1)S(1)}, f32[768,1280]{0,1:T(8,128)}) fusion(bf16[2048,1280]{1,0:T(8,128)(2,1)} %copy-done.8, bf16[768,2048]{1,0:T(8,128)(2,1)} %all-gather.2.cloned.1.call-done), kind=kOutput, calls=%fused_computation.126 | convolution fusion | flops 4027514880 | bytes 14286848 | tf_op jit(solution)/shard_map/dot_general | solution.py:148
  161.9 0.9 fusion.67
  162.8 1.2 copy-done.2
  166.0 1.2 copy.107
  167.2 0.9 copy.120
  168.1 1.1 reshape.367
  170.9 1.1 copy.149
  172.0 2.1 copy.106
  174.1 35.7 %while.17 = (s32[]{:T(128)}, f32[2,128,128]{2,1,0:T(8,128)S(1)}, f32[2,128]{1,0:T(2,128)S(1)}, f32[2]{0:T(128)S(1)}, f32[6,2,128,128]{3,2,0,1:T(8,128)}, /*index...) while((s32[]{:T(128)}, f32[2,128,128]{2,1,0:T(8,128)S(1)}, ...), condition=%wide.region_5.6_spmd.clone, body=%wide.region_0.5_spmd.clone.sunk | while | flops 202557696 | bytes 2339037 | solution.py:68
  176.7 1.4 convolution_add_fusion.4
  178.1 2.0 fusion.107
  182.6 1.4 convolution_add_fusion.4
  184.0 2.0 fusion.107
  188.6 1.4 convolution_add_fusion.4
  190.0 2.0 fusion.107
  194.5 1.4 convolution_add_fusion.4
  195.9 2.0 fusion.107
  200.5 1.4 convolution_add_fusion.4
  201.9 2.0 fusion.107
  206.4 1.4 convolution_add_fusion.4
  207.8 2.0 fusion.107
  209.8 1.5 fusion.47
  211.3 1.4 fusion.46
  213.0 2.4 %fusion.69 = (f32[6,2,128]{2,1,0:T(2,128)S(1)}, f32[6,2,128,384]{3,2,1,0:T(8,128)}) fusion(f32[2]{0:T(128)S(1)} %dynamic-slice_multiply_fusion, f32[6,2,384]{2,1,0:T(2,128)S(1)} %bitcast.189, f32[6,2,128]{2,1,0:T(2,128)S(1)} %bitcast.190, bf16[6,384,2,128]{3,2,1,0:T(2,128)(2,1)S(1)} %reshape.370, bf16[6,128,2,128]{3,2,1,0:T(2,128)(2,1)S(1)} %copy-done.5), kind=kOutput, calls=%fused_computation.127 | convolution fusion | flops 153944448 | bytes 3962888 | tf_op jit(solution)/shard_map/sub | solution.py:93
  215.4 2.8 %convolution_bitcast_fusion.1 = f32[6,128,2,128]{1,3,2,0:T(8,128)S(1)} fusion(bf16[6,384,2,128]{3,2,1,0:T(2,128)(2,1)} %reshape.366, f32[6,2,128,384]{3,2,1,0:T(8,128)} %get-tuple-element.174, f32[6,2,128]{2,1,0:T(2,128)S(1)} %get-tuple-element.173), kind=kOutput, calls=%fused_computation.65 | convolution fusion | flops 152174592 | bytes 4331520 | tf_op jit(solution)/shard_map/bhqk,bkhd->bqhd/dot_general | solution.py:95
  218.7 1.4 fusion.42
  220.2 0.9 copy.128
  (163 shorter events, 23.7 us)
Async XLA Ops:
  6.5 20.3 %copy-start = (bf16[2048,256]{1,0:T(8,128)(2,1)S(1)}, bf16[2048,256]{1,0:T(8,128)(2,1)}, u32[]{:S(2)}) copy-start(bf16[2048,256]{1,0:T(8,128)(2,1)} %param.29) | copy-start | bytes 3145732
  8.5 20.3 %all-to-all-start = ((s32[8,1,6]{2,1,0:T(1,128)}), s32[8,1,6]{2,1,0:T(1,128)S(1)}, u32[]{:S(2)}, u32[]{:S(2)}) async-start(s32[8,1,6]{2,1,0:T(1,128)} %bitcast.24), calls=%async_computation | async-start | bytes 8192 | tf_op jit(solution)/shard_map/all_to_all | solution.py:201
  15.7 4.2 %copy-start.10 = (f32[2048]{0:T(1024)S(1)}, f32[2048]{0:T(1024)}, u32[]{:S(2)}) copy-start(f32[2048]{0:T(1024)} %param.31) | copy-start | bytes 24580
  24.2 2.7 %copy-start.3 = (bf16[1536,2048]{1,0:T(8,128)(2,1)}, bf16[1536,2048]{1,0:T(8,128)(2,1)S(1)}, u32[]{:S(2)}) copy-start(bf16[1536,2048]{1,0:T(8,128)(2,1)S(1)} %fusion.33) | copy-start | bytes 18874372
  31.2 59.3 %all-to-all-start.2 = ((bf16[8,6,96,256]{3,2,1,0:T(8,128)(2,1)}), bf16[8,6,96,256]{3,2,1,0:T(8,128)(2,1)S(1)}, u32[]{:S(2)}, u32[]{:S(2)}) async-start(bf16[8,6,96,256]{3,2,1,0:T(8,128)(2,1)} %bitcast.31), calls=%async_computation.2 | async-start | bytes 4718592 | tf_op jit(solution)/shard_map/all_to_all | solution.py:206
  37.2 114.9 %all-gather.2.cloned.1.call-start = ((), (), s32[]{:S(2)}) async-start(), calls=%async_computation.3 | async-start | bytes 3932160 | tf_op jit(solution)/shard_map/all_gather | solution.py:147
  90.5 4.8 %copy-start.13 = (f32[8]{0:T(128)S(1)}, f32[8]{0:T(128)}, u32[]{:S(2)}) copy-start(f32[8]{0:T(128)} %param.32) | copy-start | bytes 100
  90.5 58.0 %all-to-all-start.1 = ((bf16[8,6,96,256]{3,2,1,0:T(8,128)(2,1)}), bf16[8,6,96,256]{3,2,1,0:T(8,128)(2,1)}, u32[]{:S(2)}, u32[]{:S(2)}) async-start(bf16[8,6,96,256]{3,2,1,0:T(8,128)(2,1)} %bitcast.26), calls=%async_computation.1 | async-start | bytes 4718592 | tf_op jit(solution)/shard_map/all_to_all | solution.py:207
  96.7 2.8 %copy-start.6 = (bf16[2048,256]{1,0:T(8,128)(2,1)S(1)}, bf16[2048,256]{1,0:T(8,128)(2,1)}, u32[]{:S(2)}) copy-start(bf16[2048,256]{1,0:T(8,128)(2,1)} %param.28) | copy-start | bytes 3145732
  98.1 1.6 copy-start.7
  99.8 2.3 %copy-start.8 = (bf16[2048,1280]{1,0:T(8,128)(2,1)}, bf16[2048,1280]{1,0:T(8,128)(2,1)S(1)}, u32[]{:S(2)}) copy-start(bf16[2048,1280]{1,0:T(8,128)(2,1)S(1)} %constant_dynamic-update-slice_fusion) | copy-start | bytes 15728644
  161.8 2.2 copy-start.2
  161.8 2.2 copy-start.9
  161.8 2.2 copy-start.11
  169.2 4.9 %copy-start.4 = (bf16[6,128,2,128]{3,2,1,0:T(2,128)(2,1)}, bf16[6,128,2,128]{3,2,1,0:T(2,128)(2,1)S(1)}, u32[]{:S(2)}) copy-start(bf16[6,128,2,128]{3,2,1,0:T(2,128)(2,1)S(1)} %reshape.367) | copy-start | bytes 1179652
  174.1 37.2 %copy-start.12 = (f32[256]{0:T(256)S(1)}, f32[256]{0:T(256)}, u32[]{:S(2)}) copy-start(f32[256]{0:T(256)} %param.27) | copy-start | bytes 3076
  209.8 3.2 %copy-start.5 = (bf16[6,128,2,128]{3,2,1,0:T(2,128)(2,1)S(1)}, bf16[6,128,2,128]{3,2,1,0:T(2,128)(2,1)}, u32[]{:S(2)}) copy-start(bf16[6,128,2,128]{3,2,1,0:T(2,128)(2,1)} %copy-done.4) | copy-start | bytes 1179652
  218.2 2.9 %copy-start.1 = (bf16[2048,256]{1,0:T(8,128)(2,1)S(1)}, bf16[2048,256]{1,0:T(8,128)(2,1)}, u32[]{:S(2)}) copy-start(bf16[2048,256]{1,0:T(8,128)(2,1)} %param.29) | copy-start | bytes 3145732
Sparse Core Ops, SparseCore 0:
  39.6 29.9 all-gather.1
where the time goes:
time: 229 us; the launch traced here: 228 us
  waiting for transfers between devices  85 us (37%)
  matrix products  48.8 us (21%)
  local copies, waits for them, and re-layouts  37.9 us (17%)
  other arithmetic  24.3 us (11%)
  starting transfers between devices  18 us (8%)
  between operations  13.7 us (6%)
    all_to_all x1, waiting for transfers between devices, local(): lax.all_to_all(shard_keys[incoming], 'st', split_axis=0, concat_axis=0, t...  45.5 us
    all_to_all x1, waiting for transfers between devices, local(): lax.all_to_all(shard_values[incoming], 'st', split_axis=0, concat_axis=0,...  38.9 us
    unnamed x36, local copies, waits for them, and re-layouts  12.7 us
    dot_general x6, matrix products, advance(): jnp.einsum('hts,hse->hte', affinity_logits, value_part, precision=HIGHEST)  11.7 us
    dot_general x1, matrix products, local(): projected = jnp.dot(token_piece, joined, preferred_element_type=jnp.float32)  9.71 us
    reduce_sum x4, other arithmetic, rms_scale(): jnp.mean(tensor * tensor, axis=-1, keepdims=True) + EPSILON  8.99 us
    dot_general x6, matrix products, advance(): jnp.einsum('hsd,hse->hde', weighted_keys, value_part, precision=HIGHEST)  8.47 us
    all_to_all x1, starting transfers between devices, local(): lax.all_to_all(outgoing, 'st', split_axis=0, concat_axis=0, tiled=True)  7.28 us
  transfers between devices with their start and end apart: 4, of which 2 were waited for; matrix products, arithmetic and copies ran while one was open for 14% of the time, Pallas kernels for 0%

commit v1 on v0

--- a/solution.py
+++ b/solution.py
@@ -1,6 +1,10 @@
+import functools
+
 import jax
 import jax.numpy as jnp
 from jax import lax
+from jax.experimental import pallas as pl
+from jax.experimental.pallas import tpu as pltpu
 from jax.sharding import PartitionSpec as P
 
 FACET_COUNT = 8
@@ -79,37 +83,157 @@
     return jnp.moveaxis(outcome, 0, 1).reshape(head_count, length, facet_dimension)
 
 
-def document_lookup_update(probe_vectors, segment_lookups, segment_contents, facet_scales):
-    facet_dimension = probe_vectors.shape[-1]
-    affinity_logits = jnp.einsum(
-        "bqhd,bkhd->bhqk", probe_vectors, segment_lookups, preferred_element_type=jnp.float32
-    )
-    ask_scale = rms_scale(probe_vectors.astype(jnp.float32))[..., 0]
-    key_scale = rms_scale(segment_lookups.astype(jnp.float32))[..., 0]
-    affinity_logits = affinity_logits * jnp.transpose(ask_scale, (0, 2, 1))[:, :, :, None]
-    affinity_logits = affinity_logits * jnp.transpose(key_scale, (0, 2, 1))[:, :, None, :]
-    affinity_logits = affinity_logits * (facet_scales / facet_dimension)[None, :, None, None]
-    peak = jnp.max(affinity_logits, axis=-1, keepdims=True)
-    exp_scores = jnp.exp(affinity_logits - peak)
-    weights = (exp_scores / jnp.sum(exp_scores, axis=-1, keepdims=True)).astype(jnp.bfloat16)
-    return jnp.einsum(
-        "bhqk,bkhd->bqhd", weights, segment_contents, preferred_element_type=jnp.float32
-    )
-
-
-def project_rows(
-    passage_rows, document_rescale_factor, document_lookup_matrix, document_content_matrix
+def store_kernel(
+    incoming, rows_ref, gain_ref, key_weight_ref, value_weight_ref, sent_ref, held, sems
 ):
-    widened = passage_rows.reshape(-1, passage_rows.shape[-1]).astype(jnp.float32)
-    normed = (widened * rms_scale(widened) * document_rescale_factor).astype(jnp.bfloat16)
-    out_shape = passage_rows.shape[:-1] + (document_lookup_matrix.shape[1],)
-    key_part = jnp.dot(normed, document_lookup_matrix, preferred_element_type=jnp.float32).astype(
-        jnp.bfloat16
-    )
-    value_part = jnp.dot(
-        normed, document_content_matrix, preferred_element_type=jnp.float32
-    ).astype(jnp.bfloat16)
-    return (key_part.reshape(out_shape), value_part.reshape(out_shape))
+    step = pl.program_id(0)
+    per_step, row_count, width = rows_ref.shape
+    half = key_weight_ref.shape[1]
+    widened = rows_ref[...].reshape(per_step * row_count, width).astype(jnp.float32)
+    normed = (widened * rms_scale(widened) * gain_ref[...]).astype(jnp.bfloat16)
+    out_shape = (per_step, row_count, half)
+    here = pl.ds(step * per_step, per_step)
+    held[here, :, :half] = (
+        jnp.dot(normed, key_weight_ref[...], preferred_element_type=jnp.float32)
+        .astype(jnp.bfloat16)
+        .reshape(out_shape)
+    )
+    held[here, :, half:] = (
+        jnp.dot(normed, value_weight_ref[...], preferred_element_type=jnp.float32)
+        .astype(jnp.bfloat16)
+        .reshape(out_shape)
+    )
+
+    @pl.when(step == pl.num_programs(0) - 1)
+    def _():
+        slot_count = sent_ref.shape[0]
+
+        def copy_of(slot):
+            return pltpu.make_async_copy(
+                held.at[incoming[slot]], sent_ref.at[slot], sems.at[slot]
+            )
+
+        def begin(slot, carry):
+            copy_of(slot).start()
+            return carry
+
+        def finish(slot, carry):
+            copy_of(slot).wait()
+            return carry
+
+        lax.fori_loop(0, slot_count, begin, 0)
+        lax.fori_loop(0, slot_count, finish, 0)
+
+
+def store_rows(
+    incoming, document_corpus, document_rescale_factor, document_lookup_matrix, document_content_matrix
+):
+    passage_count, row_count, width = document_corpus.shape
+    half = document_lookup_matrix.shape[1]
+    slots = incoming.shape[0]
+    per_step = 2
+    whole = pl.BlockSpec((width, half), lambda i, ids: (0, 0))
+    return pl.pallas_call(
+        store_kernel,
+        out_shape=jax.ShapeDtypeStruct((slots, row_count, 2 * half), jnp.bfloat16),
+        grid_spec=pltpu.PrefetchScalarGridSpec(
+            num_scalar_prefetch=1,
+            grid=(passage_count // per_step,),
+            in_specs=[
+                pl.BlockSpec((per_step, row_count, width), lambda i, ids: (i, 0, 0)),
+                pl.BlockSpec((1, width), lambda i, ids: (0, 0)),
+                whole,
+                whole,
+            ],
+            out_specs=pl.BlockSpec(memory_space=pl.ANY),
+            scratch_shapes=[
+                pltpu.VMEM((passage_count, row_count, 2 * half), jnp.bfloat16),
+                pltpu.SemaphoreType.DMA((slots,)),
+            ],
+        ),
+        compiler_params=pltpu.CompilerParams(dimension_semantics=("arbitrary",)),
+        cost_estimate=pl.CostEstimate(
+            flops=4 * passage_count * row_count * width * half,
+            bytes_accessed=2 * passage_count * row_count * width,
+            transcendentals=0,
+        ),
+    )(
+        incoming,
+        document_corpus,
+        document_rescale_factor.reshape(1, width),
+        document_lookup_matrix,
+        document_content_matrix,
+    )
+
+
+TRANS = (((1,), (1,)), ((), ()))
+
+
+def attend_kernel(reads, slot_ref, *refs):
+    passages = refs[:reads]
+    ask_ref, mix_ref, cell_ref, scale_ref, out_ref = refs[reads:]
+    width = ask_ref.shape[1]
+    facets = width // LANE_DIMENSION
+    ones = jnp.full((8, LANE_DIMENSION), 1.0, jnp.float32)
+    for facet in range(facets):
+        lanes = slice(facet * LANE_DIMENSION, (facet + 1) * LANE_DIMENSION)
+        value_lanes = slice(width + lanes.start, width + lanes.stop)
+        ask = ask_ref[:, lanes]
+        keys = jnp.concatenate([ref[0, :, lanes] for ref in passages], axis=0)
+        values = jnp.concatenate([ref[0, :, value_lanes] for ref in passages], axis=0)
+        wide_keys = keys.astype(jnp.float32)
+        squares = lax.dot_general(
+            ones, wide_keys * wide_keys, TRANS, precision=HIGHEST,
+            preferred_element_type=jnp.float32,
+        )
+        key_scale = lax.rsqrt(squares[0:1] * (1.0 / LANE_DIMENSION) + EPSILON)
+        ask_scale = rms_scale(ask.astype(jnp.float32))
+        scores = lax.dot_general(ask, keys, TRANS, preferred_element_type=jnp.float32)
+        scores = scores * ask_scale * key_scale * (scale_ref[0, facet] / LANE_DIMENSION)
+        exp_scores = jnp.exp(scores - jnp.max(scores, axis=-1, keepdims=True))
+        weights = (exp_scores / jnp.sum(exp_scores, axis=-1, keepdims=True)).astype(jnp.bfloat16)
+        found = jnp.dot(weights, values, preferred_element_type=jnp.float32)
+        out_ref[:, lanes] = (
+            cell_ref[:, lanes] + jax.nn.sigmoid(mix_ref[:, lanes]) * found
+        ).astype(jnp.bfloat16)
+
+
+def attend(slot_index, slots, ask, mix_logits, cell_out, facet_scales, block_count):
+    tok_rows, width = ask.shape
+    reads = slot_index.shape[0] // block_count
+    block_rows = tok_rows // block_count
+    row_count = slots.shape[1]
+
+    def passage_spec(place):
+        return pl.BlockSpec(
+            (1, row_count, slots.shape[2]), lambda b, ids: (ids[reads * b + place], 0, 0)
+        )
+
+    rows = pl.BlockSpec((block_rows, width), lambda b, ids: (b, 0))
+    return pl.pallas_call(
+        functools.partial(attend_kernel, reads),
+        out_shape=jax.ShapeDtypeStruct((tok_rows, width), jnp.bfloat16),
+        grid_spec=pltpu.PrefetchScalarGridSpec(
+            num_scalar_prefetch=1,
+            grid=(block_count,),
+            in_specs=[passage_spec(place) for place in range(reads)]
+            + [rows, rows, rows, pl.BlockSpec(memory_space=pltpu.SMEM)],
+            out_specs=rows,
+        ),
+        compiler_params=pltpu.CompilerParams(dimension_semantics=("arbitrary",)),
+        cost_estimate=pl.CostEstimate(
+            flops=4 * tok_rows * reads * row_count * width,
+            bytes_accessed=4 * slots.size,
+            transcendentals=tok_rows * reads * row_count,
+        ),
+    )(
+        slot_index,
+        *([slots] * reads),
+        ask,
+        mix_logits,
+        cell_out,
+        facet_scales.reshape(1, -1),
+    )
 
 
 def local(
@@ -199,25 +323,18 @@
     ).astype(jnp.int32)
     outgoing = jnp.sum(slot_hits * within[:, None], axis=0).reshape(st_devices, slot_cap)
     incoming = lax.all_to_all(outgoing, "st", split_axis=0, concat_axis=0, tiled=True)
-    shard_keys, shard_values = project_rows(
-        document_corpus, document_rescale_factor, document_lookup_matrix, document_content_matrix
-    )
-    passage_keys, passage_values = (
-        lax.all_to_all(shard_keys[incoming], "st", split_axis=0, concat_axis=0, tiled=True),
-        lax.all_to_all(shard_values[incoming], "st", split_axis=0, concat_axis=0, tiled=True),
-    )
-    slot_keys = passage_keys.reshape(st_devices * slot_cap, -1, local_width)
-    slot_values = passage_values.reshape(st_devices * slot_cap, -1, local_width)
-    segment_lookups = slot_keys[slot_index].reshape(block_count, -1, local_facets, LANE_DIMENSION)
-    segment_contents = slot_values[slot_index].reshape(
-        block_count, -1, local_facets, LANE_DIMENSION
-    )
-    segment_probes = probe_vectors.reshape(block_count, -1, local_facets, LANE_DIMENSION)
+    outgoing_rows = store_rows(
+        incoming.reshape(-1),
+        document_corpus,
+        document_rescale_factor,
+        document_lookup_matrix,
+        document_content_matrix,
+    )
+    slots = lax.all_to_all(outgoing_rows, "st", split_axis=0, concat_axis=0, tiled=True)
     facet_scales = lax.dynamic_slice_in_dim(affinity_scaling, first_facet, local_facets, 0)
-    fetched_result = document_lookup_update(
-        segment_probes, segment_lookups, segment_contents, facet_scales
-    ).reshape(tok_rows, local_width)
-    return (cell_out + jax.nn.sigmoid(mix_logits) * fetched_result).astype(jnp.bfloat16)
+    return attend(
+        slot_index, slots, probe_vectors, mix_logits, cell_out, facet_scales, block_count
+    )
 
 
 def solution(mesh):

time: 229 us -> 169 us (0.74)
  waiting for transfers between devices: 85 us -> 54.6 us
  Pallas kernels: 0 us -> 23.2 us
  local copies, waits for them, and re-layouts: 37.9 us -> 20.8 us
  matrix products: 48.8 us -> 33 us
  other arithmetic: 24.3 us -> 9.25 us
  starting transfers between devices: 18 us -> 13.2 us
    all_to_all x2 -> x1, waiting for transfers between devices: 84.3 us -> 53.9 us  [local(): lax.all_to_all(outgoing_rows, 'st', split_axis=0, concat_axis=0, tiled=True)]
    pallas_call x0 -> x2, Pallas kernels: none -> 23.2 us  [the longest x1 12.6 us: store_rows(): pl.pallas_call(store_kernel, out_shape=jax.ShapeDtypeStruct((slots, row_c...]
    dot_general x3 -> x0, matrix products: 9.53 us -> none  [the longest x1 4.84 us: project_rows(): jnp.dot(normed, document_content_matrix, preferred_element_type=jnp.float32)]
    reduce_sum x4 -> x1, other arithmetic: 8.99 us -> 0.28 us  [rms_scale(): jnp.mean(tensor * tensor, axis=-1, keepdims=True) + EPSILON]
    gather x4 -> x0, local copies, waits for them, and re-layouts: 8.52 us -> none  [the longest x1 2.29 us: local(): slot_values[slot_index]]
    convert_element_type x2 -> x0, other arithmetic: 5.71 us -> none  [the longest x1 4.27 us: project_rows(): (widened * rms_scale(widened) * document_rescale_factor).astype(jnp.bfloa...]
    unnamed x36 -> x22, local copies, waits for them, and re-layouts: 12.7 us -> 7.98 us
    all_to_all x2 -> x1, starting transfers between devices: 10.7 us -> 5.94 us  [local(): lax.all_to_all(outgoing_rows, 'st', split_axis=0, concat_axis=0, tiled=True)]
  transfers between devices with their start and end apart: 4 -> 3, of which waited for: 2 -> 1; matrix products, arithmetic and copies ran while one was open for 14% -> 37% of each run, Pallas kernels for 0% -> 7%
where the time goes in v1:
time: 169 us; the launch traced here: 168 us
  waiting for transfers between devices  54.6 us (32%)
  matrix products  33 us (20%)
  Pallas kernels  23.2 us (14%)
  local copies, waits for them, and re-layouts  20.8 us (12%)
  between operations  13.5 us (8%)
  starting transfers between devices  13.2 us (8%)
  other arithmetic  9.25 us (5%)
    all_to_all x1, waiting for transfers between devices, local(): lax.all_to_all(outgoing_rows, 'st', split_axis=0, concat_axis=0, tiled=True)  53.9 us
    pallas_call x1, Pallas kernels, store_rows(): pl.pallas_call(store_kernel, out_shape=jax.ShapeDtypeStruct((slots, row_c...  12.6 us
    pallas_call x1, Pallas kernels, attend(): pl.pallas_call(functools.partial(attend_kernel, reads), out_shape=jax.Sha...  10.6 us
    dot_general x1, matrix products, local(): projected = jnp.dot(token_piece, joined, preferred_element_type=jnp.float32)  9.7 us
    dot_general x6, matrix products, advance(): jnp.einsum('hsd,hse->hde', weighted_keys, value_part, precision=HIGHEST)  8.47 us
    unnamed x22, local copies, waits for them, and re-layouts  7.98 us
    dot_general x6, matrix products, advance(): jnp.einsum('hts,hse->hte', affinity_logits, value_part, precision=HIGHEST)  7.81 us
    all_to_all x1, starting transfers between devices, local(): lax.all_to_all(outgoing, 'st', split_axis=0, concat_axis=0, tiled=True)  7.28 us
  transfers between devices with their start and end apart: 3, of which 1 were waited for; matrix products, arithmetic and copies ran while one was open for 37% of the time, Pallas kernels for 7%

profile of v1, /device:TPU:0, one launch (start us, length us, event | category | flops | bytes accessed | tf_op | source)
XLA Modules:
  0.0 168.0 jit_solution(14161959172152885579)
XLA Ops:
  6.5 0.7 all-gather.2.cloned.1.call-update
  7.3 0.8 copy.68
  8.4 0.7 all_to_all.9
  9.1 7.3 %all-to-all-start = ((s32[8,1,6]{2,1,0:T(1,128)}), s32[8,1,6]{2,1,0:T(1,128)S(1)}, u32[]{:S(2)}, u32[]{:S(2)}) async-start(s32[8,1,6]{2,1,0:T(1,128)} %bitcast), calls=%async_computation | async-start | bytes 8192 | tf_op jit(solution)/shard_map/all_to_all | solution.py:325
  16.4 1.3 dynamic-slice_bitcast_fusion.1.refs_7_
  17.8 2.5 %constant_dynamic-update-slice_fusion.4 = bf16[2048,1280]{1,0:T(8,128)(2,1)} fusion(bf16[2048,256]{1,0:T(8,128)(2,1)} %param.21), kind=kLoop, calls=%fused_computation.71 | loop fusion | bytes 2097152
  20.2 2.5 %constant_dynamic-update-slice_fusion.3 = bf16[2048,1280]{1,0:T(8,128)(2,1)} fusion(bf16[2048,1280]{1,0:T(8,128)(2,1)} %constant_dynamic-update-slice_fusion.4, bf16[2048,256]{1,0:T(8,128)(2,1)} %param.22), kind=kLoop, calls=%fused_computation.70 | loop fusion | bytes 2097152
  22.7 1.1 constant_dynamic-update-slice_fusion.2
  23.8 1.1 constant_dynamic-update-slice_fusion.1
  24.9 1.1 constant_dynamic-update-slice_fusion
  26.1 0.5 broadcast.207
  26.6 0.7 reduce.10
  27.2 0.6 reshape.208.incoming
  27.8 12.6 %shard_map.154 = bf16[48,96,512]{2,1,0:T(8,128)(2,1)} custom-call(s32[48]{0:T(128)} %reshape.208.incoming, bf16[16,96,2048]{2,1,0:T(8,128)(2,1)} %rows_ref.1, f32[1,2048]{1,0:T(1,128)} %bitcast.155, bf16[2048,256]{1,0:T(8,128)(2,1)} %key_weight_ref.1, bf16[2048,256]{1,0:T(8,128)(2,1)} %value_weight_ref.1), custom_call_target="tpu_custom_call" | custom-call | flops 3221225472 | bytes 6291456 | tf_op jit(solution)/shard_map/pallas_call | solution.py:136
  40.4 5.9 %all-to-all-start.1 = ((bf16[48,96,512]{2,1,0:T(8,128)(2,1)}), bf16[48,96,512]{2,1,0:T(8,128)(2,1)}, u32[]{:S(2)}, u32[]{:S(2)}) async-start(bf16[48,96,512]{2,1,0:T(8,128)(2,1)} %shard_map.154), calls=%async_computation.1 | async-start | bytes 9437184 | tf_op jit(solution)/shard_map/all_to_all | solution.py:333
  46.4 9.7 %fusion.38 = (bf16[768,1280]{1,0:T(8,128)(2,1)S(1)}, f32[768,1280]{1,0:T(8,128)}) fusion(bf16[768,2048]{1,0:T(8,128)(2,1)} %all-gather.2.cloned.1.call-done, bf16[2048,1280]{1,0:T(8,128)(2,1)} %constant_dynamic-update-slice_fusion), kind=kOutput, calls=%fused_computation.86 | convolution fusion | flops 4027514880 | bytes 14286848 | tf_op jit(solution)/shard_map/dot_general | solution.py:272
  56.1 1.2 convert_bitcast_fusion
  57.3 0.9 convolution_add_fusion.2
  58.3 0.8 dynamic-slice_bitcast_fusion
  59.1 2.1 %copy_bitcast_fusion.1 = (f32[768,2,128]{2,0,1:T(8,128)S(1)}, f32[768,2,128]{2,0,1:T(8,128)}) fusion(f32[96,2,8,128]{3,2,1,0:T(8,128)S(1)} %get-tuple-element.164, f32[96,2,8,128]{3,2,1,0:T(8,128)} %get-tuple-element.165), kind=kLoop, calls=%fused_computation.51 | loop fusion | bytes 3145728 | tf_op jit(solution)/shard_map/transpose | solution.py:30
  61.2 31.9 %while.17 = (s32[]{:T(128)}, f32[2,128,128]{2,1,0:T(8,128)S(1)}, f32[2,128]{1,0:T(2,128)S(1)}, f32[2]{0:T(128)S(1)}, f32[6,2,128,128]{3,2,0,1:T(8,128)S(1)}, /*i...) while((s32[]{:T(128)}, f32[2,128,128]{2,1,0:T(8,128)S(1)}, ...), condition=%wide.region_7.8_spmd.clone, body=%wide.region_2.7_spmd.clone.sunk | while | flops 202557696 | bytes 2338518 | solution.py:72
  61.8 0.4 fusion.66
  62.2 0.3 fusion.67
  62.9 1.3 fusion.69
  64.7 1.4 convolution_add_fusion.4
  67.1 0.4 fusion.66
  67.5 0.3 fusion.67
  68.2 1.3 fusion.69
  70.0 1.4 convolution_add_fusion.4
  72.4 0.4 fusion.66
  72.8 0.3 fusion.67
  73.5 1.3 fusion.69
  75.3 1.4 convolution_add_fusion.4
  77.7 0.4 fusion.66
  78.1 0.3 fusion.67
  78.8 1.3 fusion.69
  80.6 1.4 convolution_add_fusion.4
  83.0 0.4 fusion.66
  83.4 0.3 fusion.67
  84.1 1.3 fusion.69
  86.0 1.4 convolution_add_fusion.4
  88.3 0.4 fusion.66
  89.4 1.3 fusion.69
  91.3 1.4 convolution_add_fusion.4
  93.4 2.1 %slice.38.refs_5_ = f32[768,256]{1,0:T(8,128)} slice(f32[768,1280]{1,0:T(8,128)} %get-tuple-element.172), slice={[0:768], [1024:1280]} | slice | bytes 1572864 | tf_op jit(solution)/shard_map/slice | solution.py:278
  95.7 1.0 copy_bitcast_fusion.refs_6_
  96.7 53.9 %all-to-all-done.1.refs_0_.refs_1_.refs_2_.refs_3_ = bf16[48,96,512]{2,1,0:T(8,128)(2,1)} async-done(((bf16[48,96,512]{2,1,0:T(8,128)(2,1)}), bf16[48,96,512]{2,1,0:T(8,128)(2,1)}, u32[]{:S(2)}, u32[]{:S(2)}) %all-to-all-start.1) | async-done | bytes 4718624 | tf_op jit(solution)/shard_map/all_to_all | solution.py:333
  150.6 10.6 %shard_map.155 = bf16[768,256]{1,0:T(8,128)(2,1)} custom-call(s32[24]{0:T(128)} %copy-done.7, bf16[48,96,512]{2,1,0:T(8,128)(2,1)} %all-to-all-done.1.refs_0_.refs_1_.refs_2_.refs_3_, bf16[48,96,512]{2,1,0:T(8,128)(2,1)} %all-to-all-done.1.refs_0_.refs_1_.refs_2_.refs_3_, bf16[48,96,512]{2,1,0:T(8,128)(2,1)} %all-to-all-done.1.refs_0_.refs_1_.refs_2_.refs_3_, ...), custom_call_target="tpu_custom_call" | custom-call | flops 301989888 | bytes 9437184 | tf_op jit(solution)/shard_map/pallas_call | solution.py:213
  (120 shorter events, 12.2 us)
Async XLA Ops:
  6.5 50.8 %copy-start = (bf16[2048,16]{0,1:T(8,128)(2,1)S(1)}, bf16[2048,16]{0,1:T(8,128)(2,1)}, u32[]{:S(2)}) copy-start(bf16[2048,16]{0,1:T(8,128)(2,1)} %param.24) | copy-start | bytes 196612
  6.5 16.2 %copy-start.2 = (bf16[2048,256]{1,0:T(8,128)(2,1)S(1)}, bf16[2048,256]{1,0:T(8,128)(2,1)}, u32[]{:S(2)}) copy-start(bf16[2048,256]{1,0:T(8,128)(2,1)} %param.23) | copy-start | bytes 3145732
  6.5 17.3 %copy-start.3 = (bf16[2048,256]{1,0:T(8,128)(2,1)S(1)}, bf16[2048,256]{1,0:T(8,128)(2,1)}, u32[]{:S(2)}) copy-start(bf16[2048,256]{1,0:T(8,128)(2,1)} %param.28) | copy-start | bytes 3145732
  6.5 39.8 %all-gather.2.cloned.1.call-start = ((), (), s32[]{:S(2)}) async-start(), calls=%async_computation.2 | async-start | bytes 3932160 | tf_op jit(solution)/shard_map/all_gather | solution.py:271
  8.3 17.7 %copy-start.7 = (s32[24]{0:T(128)}, s32[24]{0:T(128)S(1)}, u32[]{:S(2)}) copy-start(s32[24]{0:T(128)S(1)} %multiply_add_fusion.1.slot_ref) | copy-start | bytes 292
  9.1 17.0 %all-to-all-start = ((s32[8,1,6]{2,1,0:T(1,128)}), s32[8,1,6]{2,1,0:T(1,128)S(1)}, u32[]{:S(2)}, u32[]{:S(2)}) async-start(s32[8,1,6]{2,1,0:T(1,128)} %bitcast), calls=%async_computation | async-start | bytes 8192 | tf_op jit(solution)/shard_map/all_to_all | solution.py:325
  16.4 8.5 %copy-start.4 = (bf16[2048,256]{1,0:T(8,128)(2,1)S(1)}, bf16[2048,256]{1,0:T(8,128)(2,1)}, u32[]{:S(2)}) copy-start(bf16[2048,256]{1,0:T(8,128)(2,1)} %param.33) | copy-start | bytes 3145732
  40.4 110.2 %all-to-all-start.1 = ((bf16[48,96,512]{2,1,0:T(8,128)(2,1)}), bf16[48,96,512]{2,1,0:T(8,128)(2,1)}, u32[]{:S(2)}, u32[]{:S(2)}) async-start(bf16[48,96,512]{2,1,0:T(8,128)(2,1)} %shard_map.154), calls=%async_computation.1 | async-start | bytes 9437184 | tf_op jit(solution)/shard_map/all_to_all | solution.py:333
  46.3 11.0 %copy-start.5 = (f32[16]{0:T(128)S(1)}, f32[16]{0:T(128)}, u32[]{:S(2)}) copy-start(f32[16]{0:T(128)} %param.25) | copy-start | bytes 196
  46.4 11.0 %copy-start.1 = (bf16[768,2048]{1,0:T(8,128)(2,1)S(1)}, bf16[768,2048]{1,0:T(8,128)(2,1)}, u32[]{:S(2)}) copy-start(bf16[768,2048]{1,0:T(8,128)(2,1)} %all-gather.2.cloned.1.call-done) | copy-start | bytes 9437188
  61.2 34.2 %copy-start.6 = (f32[256]{0:T(256)S(1)}, f32[256]{0:T(256)}, u32[]{:S(2)}) copy-start(f32[256]{0:T(256)} %param.27) | copy-start | bytes 3076
Sparse Core Ops, SparseCore 0:
  8.9 31.2 all-gather.1

commit v2 on v1

--- a/solution.py
+++ b/solution.py
@@ -174,7 +174,7 @@
     ask_ref, mix_ref, cell_ref, scale_ref, out_ref = refs[reads:]
     width = ask_ref.shape[1]
     facets = width // LANE_DIMENSION
-    ones = jnp.full((8, LANE_DIMENSION), 1.0, jnp.float32)
+    ones = jnp.full((8, LANE_DIMENSION), 1.0, jnp.bfloat16)
     for facet in range(facets):
         lanes = slice(facet * LANE_DIMENSION, (facet + 1) * LANE_DIMENSION)
         value_lanes = slice(width + lanes.start, width + lanes.stop)
@@ -182,10 +182,12 @@
         keys = jnp.concatenate([ref[0, :, lanes] for ref in passages], axis=0)
         values = jnp.concatenate([ref[0, :, value_lanes] for ref in passages], axis=0)
         wide_keys = keys.astype(jnp.float32)
+        squared = wide_keys * wide_keys
+        high = squared.astype(jnp.bfloat16)
+        low = (squared - high.astype(jnp.float32)).astype(jnp.bfloat16)
         squares = lax.dot_general(
-            ones, wide_keys * wide_keys, TRANS, precision=HIGHEST,
-            preferred_element_type=jnp.float32,
-        )
+            ones, high, TRANS, preferred_element_type=jnp.float32
+        ) + lax.dot_general(ones, low, TRANS, preferred_element_type=jnp.float32)
         key_scale = lax.rsqrt(squares[0:1] * (1.0 / LANE_DIMENSION) + EPSILON)
         ask_scale = rms_scale(ask.astype(jnp.float32))
         scores = lax.dot_general(ask, keys, TRANS, preferred_element_type=jnp.float32)
@@ -234,6 +236,21 @@
         cell_out,
         facet_scales.reshape(1, -1),
     )
+
+
+def gather_features(piece):
+    count = lax.axis_size("tp")
+    me = lax.axis_index("tp")
+    pieces = [piece]
+    for shift in range(1, count):
+        pairs = [((i + shift) % count, i) for i in range(count)]
+        pieces.append(lax.ppermute(piece, "tp", pairs))
+    stacked = jnp.stack(pieces)
+    ordered = [
+        lax.dynamic_index_in_dim(stacked, lax.rem(i - me + count, count), 0, keepdims=False)
+        for i in range(count)
+    ]
+    return jnp.concatenate(ordered, axis=1)
 
 
 def local(
@@ -258,52 +275,6 @@
     local_width = memory_probe_matrix.shape[1]
     local_facets = local_width // LANE_DIMENSION
     tok_rows = symbol_activations.shape[0]
-    joined = jnp.concatenate(
-        [
-            memory_probe_matrix,
-            memory_lookup_matrix,
-            memory_content_matrix,
-            document_probe_matrix,
-            fetched_mixer_matrix,
-        ],
-        axis=1,
-    )
-    token_piece = lax.all_gather(symbol_activations, "tp", axis=1, tiled=True)
-    projected = jnp.dot(token_piece, joined, preferred_element_type=jnp.float32)
-    gate_preactivation = jnp.dot(token_piece, valve_matrix, preferred_element_type=jnp.float32)
-    queries = projected[:, :local_width].astype(jnp.bfloat16)
-    key_rows = projected[:, local_width : 2 * local_width].astype(jnp.bfloat16)
-    value_rows = projected[:, 2 * local_width : 3 * local_width].astype(jnp.bfloat16)
-    probe_vectors = projected[:, 3 * local_width : 4 * local_width].astype(jnp.bfloat16)
-    mix_logits = projected[:, 4 * local_width :]
-    first_facet = head_index * local_facets
-    gate_preactivation = gate_preactivation + valve_biases
-    input_logits = lax.dynamic_slice_in_dim(gate_preactivation, first_facet, local_facets, 1)
-    forget_logits = lax.dynamic_slice_in_dim(
-        gate_preactivation, FACET_COUNT + first_facet, local_facets, 1
-    )
-    forget_log_gate = jax.nn.log_sigmoid(forget_logits) + lax.dynamic_slice_in_dim(
-        added_decay_logit, first_facet, local_facets, 1
-    )
-
-    def heads_first(tensor):
-        return jnp.transpose(
-            tensor.astype(jnp.float32).reshape(tok_rows, local_facets, LANE_DIMENSION), (1, 0, 2)
-        )
-
-    cell_out = cell_blocks(
-        heads_first(queries),
-        heads_first(key_rows),
-        heads_first(value_rows),
-        input_logits.T,
-        forget_log_gate.T,
-    )
-    cell_out = (
-        cell_out
-        * rms_scale(cell_out)
-        * facet_rescale_factor.reshape(local_facets, 1, LANE_DIMENSION)
-    )
-    cell_out = jnp.transpose(cell_out, (1, 0, 2)).reshape(tok_rows, local_width)
     st_devices = lax.axis_size("st")
     flat_ids = document_choice_matrix.reshape(-1)
     request_count = flat_ids.shape[0]
@@ -330,6 +301,71 @@
         document_lookup_matrix,
         document_content_matrix,
     )
+    (
+        outgoing_rows,
+        symbol_activations,
+        memory_probe_matrix,
+        memory_lookup_matrix,
+        memory_content_matrix,
+        document_probe_matrix,
+        fetched_mixer_matrix,
+    ) = lax.optimization_barrier(
+        (
+            outgoing_rows,
+            symbol_activations,
+            memory_probe_matrix,
+            memory_lookup_matrix,
+            memory_content_matrix,
+            document_probe_matrix,
+            fetched_mixer_matrix,
+        )
+    )
+    joined = jnp.concatenate(
+        [
+            memory_probe_matrix,
+            memory_lookup_matrix,
+            memory_content_matrix,
+            document_probe_matrix,
+            fetched_mixer_matrix,
+        ],
+        axis=1,
+    )
+    token_piece = gather_features(symbol_activations)
+    projected = jnp.dot(token_piece, joined, preferred_element_type=jnp.float32)
+    gate_preactivation = jnp.dot(token_piece, valve_matrix, preferred_element_type=jnp.float32)
+    queries = projected[:, :local_width].astype(jnp.bfloat16)
+    key_rows = projected[:, local_width : 2 * local_width].astype(jnp.bfloat16)
+    value_rows = projected[:, 2 * local_width : 3 * local_width].astype(jnp.bfloat16)
+    probe_vectors = projected[:, 3 * local_width : 4 * local_width].astype(jnp.bfloat16)
+    mix_logits = projected[:, 4 * local_width :]
+    first_facet = head_index * local_facets
+    gate_preactivation = gate_preactivation + valve_biases
+    input_logits = lax.dynamic_slice_in_dim(gate_preactivation, first_facet, local_facets, 1)
+    forget_logits = lax.dynamic_slice_in_dim(
+        gate_preactivation, FACET_COUNT + first_facet, local_facets, 1
+    )
+    forget_log_gate = jax.nn.log_sigmoid(forget_logits) + lax.dynamic_slice_in_dim(
+        added_decay_logit, first_facet, local_facets, 1
+    )
+
+    def heads_first(tensor):
+        return jnp.transpose(
+            tensor.astype(jnp.float32).reshape(tok_rows, local_facets, LANE_DIMENSION), (1, 0, 2)
+        )
+
+    cell_out = cell_blocks(
+        heads_first(queries),
+        heads_first(key_rows),
+        heads_first(value_rows),
+        input_logits.T,
+        forget_log_gate.T,
+    )
+    cell_out = (
+        cell_out
+        * rms_scale(cell_out)
+        * facet_rescale_factor.reshape(local_facets, 1, LANE_DIMENSION)
+    )
+    cell_out = jnp.transpose(cell_out, (1, 0, 2)).reshape(tok_rows, local_width)
     slots = lax.all_to_all(outgoing_rows, "st", split_axis=0, concat_axis=0, tiled=True)
     facet_scales = lax.dynamic_slice_in_dim(affinity_scaling, first_facet, local_facets, 0)
     return attend(

time: 169 us -> 151 us (0.89)
  between operations: 13.5 us -> 0.27 us
  local copies, waits for them, and re-layouts: 20.8 us -> 14.5 us
  waiting for transfers between devices: 54.6 us -> 58.4 us
  matrix products: 33 us -> 29.5 us
  other arithmetic: 9.25 us -> 11 us
  starting transfers between devices: 13.2 us -> 14.9 us
  Pallas kernels: 23.2 us -> 21.5 us
    all_to_all x1, waiting for transfers between devices: 53.9 us -> 26.8 us  [local(): lax.all_to_all(outgoing_rows, 'st', split_axis=0, concat_axis=0, tiled=True)]
    ppermute x0 -> x3, waiting for transfers between devices: none -> 26.5 us  [gather_features(): pieces.append(lax.ppermute(piece, 'tp', pairs))]
    unnamed x22 -> x24, local copies, waits for them, and re-layouts: 7.98 us -> 2.63 us
    all_to_all x1, waiting for transfers between devices: 0.01 us -> 5.13 us  [local(): lax.all_to_all(outgoing, 'st', split_axis=0, concat_axis=0, tiled=True)]
    dot_general x1, matrix products: 9.7 us -> 6.18 us  [local(): projected = jnp.dot(token_piece, joined, preferred_element_type=jnp.float32)]
    ppermute x0 -> x3, starting transfers between devices: none -> 3.03 us  [gather_features(): pieces.append(lax.ppermute(piece, 'tp', pairs))]
    another operation x0 -> x1, other arithmetic: none -> 1.8 us  [gather_features(): stacked = jnp.stack(pieces)]
  transfers between devices with their start and end apart: 3 -> 5, of which waited for: 1 -> 5; matrix products, arithmetic and copies ran while one was open for 37% -> 34% of each run, Pallas kernels for 7% -> 0%
where the time goes in v2:
time: 151 us; the launch traced here: 150 us
  waiting for transfers between devices  58.4 us (39%)
  matrix products  29.5 us (20%)
  Pallas kernels  21.5 us (14%)
  starting transfers between devices  14.9 us (10%)
  local copies, waits for them, and re-layouts  14.5 us (10%)
  other arithmetic  11 us (7%)
    all_to_all x1, waiting for transfers between devices, local(): lax.all_to_all(outgoing_rows, 'st', split_axis=0, concat_axis=0, tiled=True)  26.8 us
    ppermute x3, waiting for transfers between devices, gather_features(): pieces.append(lax.ppermute(piece, 'tp', pairs))  26.5 us
    pallas_call x1, Pallas kernels, store_rows(): pl.pallas_call(store_kernel, out_shape=jax.ShapeDtypeStruct((slots, row_c...  12.4 us
    pallas_call x1, Pallas kernels, attend(): pl.pallas_call(functools.partial(attend_kernel, reads), out_shape=jax.Sha...  9.06 us
    dot_general x6, matrix products, advance(): jnp.einsum('hsd,hse->hde', weighted_keys, value_part, precision=HIGHEST)  8.47 us
    dot_general x6, matrix products, advance(): jnp.einsum('hts,hse->hte', affinity_logits, value_part, precision=HIGHEST)  7.79 us
    all_to_all x1, starting transfers between devices, local(): lax.all_to_all(outgoing, 'st', split_axis=0, concat_axis=0, tiled=True)  7.28 us
    dot_general x1, matrix products, local(): projected = jnp.dot(token_piece, joined, preferred_element_type=jnp.float32)  6.18 us
  transfers between devices with their start and end apart: 5, of which 5 were waited for; matrix products, arithmetic and copies ran while one was open for 34% of the time, Pallas kernels for 0%

profile of v2, /device:TPU:0, one launch (start us, length us, event | category | flops | bytes accessed | tf_op | source)
XLA Modules:
  0.0 150.5 jit_solution(6909405558754346714)
XLA Ops:
  0.0 0.8 copy.64
  1.2 0.7 all_to_all.9
  1.9 7.3 %all-to-all-start = ((s32[8,1,6]{2,1,0:T(1,128)}), s32[8,1,6]{2,1,0:T(1,128)S(1)}, u32[]{:S(2)}, u32[]{:S(2)}) async-start(s32[8,1,6]{2,1,0:T(1,128)} %bitcast), calls=%async_computation | async-start | bytes 8192 | tf_op jit(solution)/shard_map/all_to_all | solution.py:296
  9.2 1.3 dynamic-slice_bitcast_fusion.5.refs_7_
  10.4 5.1 %all-to-all-done = s32[8,1,6]{2,1,0:T(1,128)S(1)} async-done(((s32[8,1,6]{2,1,0:T(1,128)}), s32[8,1,6]{2,1,0:T(1,128)S(1)}, u32[]{:S(2)}, u32[]{:S(2)}) %all-to-all-start) | async-done | bytes 224 | tf_op jit(solution)/shard_map/all_to_all | solution.py:296
  15.6 0.5 broadcast.215
  16.1 0.7 reduce.10
  16.7 0.6 reshape.208.incoming
  17.3 12.4 %shard_map.154 = bf16[48,96,512]{2,1,0:T(8,128)(2,1)} custom-call(s32[48]{0:T(128)} %reshape.208.incoming, bf16[16,96,2048]{2,1,0:T(8,128)(2,1)} %rows_ref.1, f32[1,2048]{1,0:T(1,128)} %bitcast.164, bf16[2048,256]{1,0:T(8,128)(2,1)} %key_weight_ref.1, bf16[2048,256]{1,0:T(8,128)(2,1)} %value_weight_ref.1), custom_call_target="tpu_custom_call" | custom-call | flops 3221225472 | bytes 6291456 | tf_op jit(solution)/shard_map/pallas_call | solution.py:136
  29.9 1.6 %collective-permute-start.1 = (bf16[768,512]{1,0:T(8,128)(2,1)}, bf16[768,512]{1,0:T(8,128)(2,1)}, u32[]{:S(2)}, u32[]{:S(2)}) collective-permute-start(bf16[768,512]{1,0:T(8,128)(2,1)} %param.18), channel_id=1, source_target_pairs={{2,0},{3,1},{0,2},{1,3},{6,4},{7,5},{4,6},{5,7},{10,8},{11,9},{8,1... | collective-permute-start | bytes 2359304 | tf_op jit(solution)/shard_map/ppermute | solution.py:247
  31.4 1.4 collective-permute-start
  32.8 4.6 %all-to-all-start.1 = ((bf16[48,96,512]{2,1,0:T(8,128)(2,1)}), bf16[48,96,512]{2,1,0:T(8,128)(2,1)}, u32[]{:S(2)}, u32[]{:S(2)}) async-start(bf16[48,96,512]{2,1,0:T(8,128)(2,1)} %shard_map.154), calls=%async_computation.1 | async-start | bytes 9437184 | tf_op jit(solution)/shard_map/all_to_all | solution.py:369
  37.7 1.4 constant_dynamic-update-slice_fusion.2
  39.4 9.9 %collective-permute-done.2 = bf16[768,512]{1,0:T(8,128)(2,1)} collective-permute-done((bf16[768,512]{1,0:T(8,128)(2,1)}, bf16[768,512]{1,0:T(8,128)(2,1)}, u32[]{:S(2)}, u32[]{:S(2)}) %collective-permute-start.2) | collective-permute-done | bytes 786464 | tf_op jit(solution)/shard_map/ppermute | solution.py:247
  49.3 1.3 collective-permute-done.1
  50.6 15.2 %collective-permute-done = bf16[768,512]{1,0:T(8,128)(2,1)} collective-permute-done((bf16[768,512]{1,0:T(8,128)(2,1)}, bf16[768,512]{1,0:T(8,128)(2,1)}, u32[]{:S(2)}, u32[]{:S(2)}) %collective-permute-start) | collective-permute-done | bytes 786464 | tf_op jit(solution)/shard_map/ppermute | solution.py:247
  65.9 1.8 %pad_maximum_fusion = bf16[4,768,512]{2,1,0:T(8,128)(2,1)S(1)} fusion(bf16[1,768,512]{2,1,0:T(8,128)(2,1)} %bitcast.5, bf16[1,768,512]{2,1,0:T(8,128)(2,1)} %bitcast.4, bf16[1,768,512]{2,1,0:T(8,128)(2,1)} %bitcast.3, bf16[1,768,512]{2,1,0:T(8,128)(2,1)S(1)} %bitcast.154), kind=kLoop, calls=%fused_computation.48 | loop fusion | flops 4718592 | bytes 6291456 | tf_op jit(solution)/shard_map/stack | solution.py:248
  67.9 6.2 %fusion.41 = (bf16[768,1280]{1,0:T(8,128)(2,1)S(1)}, f32[768,1280]{1,0:T(8,128)}) fusion(bf16[2048,1280]{1,0:T(8,128)(2,1)S(1)} %constant_dynamic-update-slice_fusion, bf16[768,512]{1,0:T(8,128)(2,1)S(1)} %get-tuple-element.179, bf16[768,512]{1,0:T(8,128)(2,1)S(1)} %get-tuple-element.180, bf16[768,512]{1,0:T(8,128)(2,1)S(1)} %get-tuple-element.181, ...), kind=kOutput, calls=%fused_computation.94 | convolution fusion | flops 4040097792 | bytes 14286848 | tf_op jit(solution)/shard_map/dot_general | solution.py:334
  74.1 1.1 convert_bitcast_fusion
  75.3 0.9 convolution_add_fusion.2
  76.3 0.8 dynamic-slice_bitcast_fusion.4
  77.1 2.1 %copy_bitcast_fusion.1 = (f32[768,2,128]{2,0,1:T(8,128)S(1)}, f32[768,2,128]{2,0,1:T(8,128)}) fusion(f32[96,2,8,128]{3,2,1,0:T(8,128)S(1)} %get-tuple-element.182, f32[96,2,8,128]{3,2,1,0:T(8,128)} %get-tuple-element.183), kind=kLoop, calls=%fused_computation.52 | loop fusion | bytes 3145728 | tf_op jit(solution)/shard_map/transpose | solution.py:30
  79.2 31.9 %while.17 = (s32[]{:T(128)}, f32[2,128,128]{2,1,0:T(8,128)S(1)}, f32[2,128]{1,0:T(2,128)S(1)}, f32[2]{0:T(128)S(1)}, f32[6,2,128,128]{3,2,0,1:T(8,128)S(1)}, /*i...) while((s32[]{:T(128)}, f32[2,128,128]{2,1,0:T(8,128)S(1)}, ...), condition=%wide.region_7.8_spmd.clone, body=%wide.region_2.7_spmd.clone.sunk | while | flops 202557696 | bytes 2339037 | solution.py:72
  79.7 0.4 fusion.67
  80.2 0.3 fusion.68
  81.4 1.4 convolution_add_fusion.4
  83.2 1.3 fusion.70
  85.1 0.4 fusion.67
  85.5 0.3 fusion.68
  86.7 1.4 convolution_add_fusion.4
  88.5 1.3 fusion.70
  90.4 0.4 fusion.67
  90.8 0.3 fusion.68
  92.0 1.4 convolution_add_fusion.4
  93.8 1.3 fusion.70
  95.7 0.4 fusion.67
  97.3 1.4 convolution_add_fusion.4
  99.1 1.3 fusion.70
  101.0 0.4 fusion.67
  102.6 1.4 convolution_add_fusion.4
  104.4 1.3 fusion.70
  106.3 0.4 fusion.67
  108.0 1.4 convolution_add_fusion.4
  109.7 1.3 fusion.70
  111.1 2.1 %slice.38.refs_5_ = f32[768,256]{1,0:T(8,128)} slice(f32[768,1280]{1,0:T(8,128)} %get-tuple-element.190), slice={[0:768], [1024:1280]} | slice | bytes 1572864 | tf_op jit(solution)/shard_map/slice | solution.py:340
  113.7 0.9 copy_bitcast_fusion.refs_6_
  114.7 26.8 %all-to-all-done.1.refs_0_.refs_1_.refs_2_.refs_3_ = bf16[48,96,512]{2,1,0:T(8,128)(2,1)} async-done(((bf16[48,96,512]{2,1,0:T(8,128)(2,1)}), bf16[48,96,512]{2,1,0:T(8,128)(2,1)}, u32[]{:S(2)}, u32[]{:S(2)}) %all-to-all-start.1) | async-done | bytes 4718624 | tf_op jit(solution)/shard_map/all_to_all | solution.py:369
  141.4 9.1 %shard_map.155 = bf16[768,256]{1,0:T(8,128)(2,1)} custom-call(s32[24]{0:T(128)} %copy-done.7, bf16[48,96,512]{2,1,0:T(8,128)(2,1)} %all-to-all-done.1.refs_0_.refs_1_.refs_2_.refs_3_, bf16[48,96,512]{2,1,0:T(8,128)(2,1)} %all-to-all-done.1.refs_0_.refs_1_.refs_2_.refs_3_, bf16[48,96,512]{2,1,0:T(8,128)(2,1)} %all-to-all-done.1.refs_0_.refs_1_.refs_2_.refs_3_, ...), custom_call_target="tpu_custom_call" | custom-call | flops 301989888 | bytes 9437184 | tf_op jit(solution)/shard_map/pallas_call | solution.py:215
  (127 shorter events, 13.4 us)
Async XLA Ops:
  0.0 75.3 %copy-start = (bf16[2048,16]{0,1:T(8,128)(2,1)S(1)}, bf16[2048,16]{0,1:T(8,128)(2,1)}, u32[]{:S(2)}) copy-start(bf16[2048,16]{0,1:T(8,128)(2,1)} %param.24) | copy-start | bytes 196612
  1.1 28.7 %copy-start.7 = (s32[24]{0:T(128)}, s32[24]{0:T(128)S(1)}, u32[]{:S(2)}) copy-start(s32[24]{0:T(128)S(1)} %multiply_add_fusion.1.slot_ref) | copy-start | bytes 292
  1.9 13.7 %all-to-all-start = ((s32[8,1,6]{2,1,0:T(1,128)}), s32[8,1,6]{2,1,0:T(1,128)S(1)}, u32[]{:S(2)}, u32[]{:S(2)}) async-start(s32[8,1,6]{2,1,0:T(1,128)} %bitcast), calls=%async_computation | async-start | bytes 8192 | tf_op jit(solution)/shard_map/all_to_all | solution.py:296
  29.8 7.7 %copy-start.1 = (bf16[2048,256]{1,0:T(8,128)(2,1)S(1)}, bf16[2048,256]{1,0:T(8,128)(2,1)}, u32[]{:S(2)}) copy-start(bf16[2048,256]{1,0:T(8,128)(2,1)} %param.21) | copy-start | bytes 3145732
  29.8 7.8 %copy-start.2 = (bf16[2048,256]{1,0:T(8,128)(2,1)S(1)}, bf16[2048,256]{1,0:T(8,128)(2,1)}, u32[]{:S(2)}) copy-start(bf16[2048,256]{1,0:T(8,128)(2,1)} %param.22) | copy-start | bytes 3145732
  29.8 19.6 %collective-permute-start.2 = (bf16[768,512]{1,0:T(8,128)(2,1)}, bf16[768,512]{1,0:T(8,128)(2,1)}, u32[]{:S(2)}, u32[]{:S(2)}) collective-permute-start(bf16[768,512]{1,0:T(8,128)(2,1)} %param.18), channel_id=1, source_target_pairs={{3,0},{0,1},{1,2},{2,3},{7,4},{4,5},{5,6},{6,7},{11,8},{8,9},{9,10... | collective-permute-start | bytes 2359304 | tf_op jit(solution)/shard_map/ppermute | solution.py:247
  29.9 20.8 %collective-permute-start.1 = (bf16[768,512]{1,0:T(8,128)(2,1)}, bf16[768,512]{1,0:T(8,128)(2,1)}, u32[]{:S(2)}, u32[]{:S(2)}) collective-permute-start(bf16[768,512]{1,0:T(8,128)(2,1)} %param.18), channel_id=1, source_target_pairs={{2,0},{3,1},{0,2},{1,3},{6,4},{7,5},{4,6},{5,7},{10,8},{11,9},{8,1... | collective-permute-start | bytes 2359304 | tf_op jit(solution)/shard_map/ppermute | solution.py:247
  31.4 34.4 %collective-permute-start = (bf16[768,512]{1,0:T(8,128)(2,1)}, bf16[768,512]{1,0:T(8,128)(2,1)}, u32[]{:S(2)}, u32[]{:S(2)}) collective-permute-start(bf16[768,512]{1,0:T(8,128)(2,1)} %param.18), channel_id=1, source_target_pairs={{1,0},{2,1},{3,2},{0,3},{5,4},{6,5},{7,6},{4,7},{9,8},{10,9},{11,1... | collective-permute-start | bytes 2359304 | tf_op jit(solution)/shard_map/ppermute | solution.py:247
  32.8 108.6 %all-to-all-start.1 = ((bf16[48,96,512]{2,1,0:T(8,128)(2,1)}), bf16[48,96,512]{2,1,0:T(8,128)(2,1)}, u32[]{:S(2)}, u32[]{:S(2)}) async-start(bf16[48,96,512]{2,1,0:T(8,128)(2,1)} %shard_map.154), calls=%async_computation.1 | async-start | bytes 9437184 | tf_op jit(solution)/shard_map/all_to_all | solution.py:369
  37.5 1.7 %copy-start.3 = (bf16[2048,256]{1,0:T(8,128)(2,1)S(1)}, bf16[2048,256]{1,0:T(8,128)(2,1)}, u32[]{:S(2)}) copy-start(bf16[2048,256]{1,0:T(8,128)(2,1)} %param.28) | copy-start | bytes 3145732
  37.5 1.8 %copy-start.4 = (bf16[2048,256]{1,0:T(8,128)(2,1)S(1)}, bf16[2048,256]{1,0:T(8,128)(2,1)}, u32[]{:S(2)}) copy-start(bf16[2048,256]{1,0:T(8,128)(2,1)} %param.33) | copy-start | bytes 3145732
  37.5 28.4 %copy-start.5 = (bf16[768,512]{1,0:T(8,128)(2,1)S(1)}, bf16[768,512]{1,0:T(8,128)(2,1)}, u32[]{:S(2)}) copy-start(bf16[768,512]{1,0:T(8,128)(2,1)} %param.18) | copy-start | bytes 2359300
  67.9 7.4 %copy-start.8 = (f32[16]{0:T(128)S(1)}, f32[16]{0:T(128)}, u32[]{:S(2)}) copy-start(f32[16]{0:T(128)} %param.25) | copy-start | bytes 196
  79.2 34.2 %copy-start.6 = (f32[256]{0:T(256)S(1)}, f32[256]{0:T(256)}, u32[]{:S(2)}) copy-start(f32[256]{0:T(256)} %param.27) | copy-start | bytes 3076

commit v3 on v2

--- a/solution.py
+++ b/solution.py
@@ -83,74 +83,42 @@
     return jnp.moveaxis(outcome, 0, 1).reshape(head_count, length, facet_dimension)
 
 
-def store_kernel(
-    incoming, rows_ref, gain_ref, key_weight_ref, value_weight_ref, sent_ref, held, sems
-):
-    step = pl.program_id(0)
+def store_kernel(rows_ref, gain_ref, key_weight_ref, value_weight_ref, out_ref):
     per_step, row_count, width = rows_ref.shape
     half = key_weight_ref.shape[1]
     widened = rows_ref[...].reshape(per_step * row_count, width).astype(jnp.float32)
     normed = (widened * rms_scale(widened) * gain_ref[...]).astype(jnp.bfloat16)
     out_shape = (per_step, row_count, half)
-    here = pl.ds(step * per_step, per_step)
-    held[here, :, :half] = (
+    out_ref[:, :, :half] = (
         jnp.dot(normed, key_weight_ref[...], preferred_element_type=jnp.float32)
         .astype(jnp.bfloat16)
         .reshape(out_shape)
     )
-    held[here, :, half:] = (
+    out_ref[:, :, half:] = (
         jnp.dot(normed, value_weight_ref[...], preferred_element_type=jnp.float32)
         .astype(jnp.bfloat16)
         .reshape(out_shape)
     )
 
-    @pl.when(step == pl.num_programs(0) - 1)
-    def _():
-        slot_count = sent_ref.shape[0]
-
-        def copy_of(slot):
-            return pltpu.make_async_copy(
-                held.at[incoming[slot]], sent_ref.at[slot], sems.at[slot]
-            )
-
-        def begin(slot, carry):
-            copy_of(slot).start()
-            return carry
-
-        def finish(slot, carry):
-            copy_of(slot).wait()
-            return carry
-
-        lax.fori_loop(0, slot_count, begin, 0)
-        lax.fori_loop(0, slot_count, finish, 0)
-
 
 def store_rows(
-    incoming, document_corpus, document_rescale_factor, document_lookup_matrix, document_content_matrix
+    document_corpus, document_rescale_factor, document_lookup_matrix, document_content_matrix
 ):
     passage_count, row_count, width = document_corpus.shape
     half = document_lookup_matrix.shape[1]
-    slots = incoming.shape[0]
     per_step = 2
-    whole = pl.BlockSpec((width, half), lambda i, ids: (0, 0))
+    whole = pl.BlockSpec((width, half), lambda i: (0, 0))
     return pl.pallas_call(
         store_kernel,
-        out_shape=jax.ShapeDtypeStruct((slots, row_count, 2 * half), jnp.bfloat16),
-        grid_spec=pltpu.PrefetchScalarGridSpec(
-            num_scalar_prefetch=1,
-            grid=(passage_count // per_step,),
-            in_specs=[
-                pl.BlockSpec((per_step, row_count, width), lambda i, ids: (i, 0, 0)),
-                pl.BlockSpec((1, width), lambda i, ids: (0, 0)),
-                whole,
-                whole,
-            ],
-            out_specs=pl.BlockSpec(memory_space=pl.ANY),
-            scratch_shapes=[
-                pltpu.VMEM((passage_count, row_count, 2 * half), jnp.bfloat16),
-                pltpu.SemaphoreType.DMA((slots,)),
-            ],
-        ),
+        out_shape=jax.ShapeDtypeStruct((passage_count, row_count, 2 * half), jnp.bfloat16),
+        grid=(passage_count // per_step,),
+        in_specs=[
+            pl.BlockSpec((per_step, row_count, width), lambda i: (i, 0, 0)),
+            pl.BlockSpec((1, width), lambda i: (0, 0)),
+            whole,
+            whole,
+        ],
+        out_specs=pl.BlockSpec((per_step, row_count, 2 * half), lambda i: (i, 0, 0)),
         compiler_params=pltpu.CompilerParams(dimension_semantics=("arbitrary",)),
         cost_estimate=pl.CostEstimate(
             flops=4 * passage_count * row_count * width * half,
@@ -158,12 +126,46 @@
             transcendentals=0,
         ),
     )(
-        incoming,
         document_corpus,
         document_rescale_factor.reshape(1, width),
         document_lookup_matrix,
         document_content_matrix,
     )
+
+
+def pick_kernel(incoming, held, sent_ref, sems):
+    slot_count = sent_ref.shape[0]
+
+    def copy_of(slot):
+        return pltpu.make_async_copy(
+            held.at[incoming[slot]], sent_ref.at[slot], sems.at[slot]
+        )
+
+    def begin(slot, carry):
+        copy_of(slot).start()
+        return carry
+
+    def finish(slot, carry):
+        copy_of(slot).wait()
+        return carry
+
+    lax.fori_loop(0, slot_count, begin, 0)
+    lax.fori_loop(0, slot_count, finish, 0)
+
+
+def pick_rows(incoming, store):
+    slots = incoming.shape[0]
+    shape = (slots,) + store.shape[1:]
+    return pl.pallas_call(
+        pick_kernel,
+        out_shape=jax.ShapeDtypeStruct(shape, store.dtype),
+        in_specs=[
+            pl.BlockSpec(memory_space=pltpu.SMEM),
+            pl.BlockSpec(memory_space=pltpu.VMEM),
+        ],
+        out_specs=pl.BlockSpec(memory_space=pl.ANY),
+        scratch_shapes=[pltpu.SemaphoreType.DMA((slots,))],
+    )(incoming, store)
 
 
 TRANS = (((1,), (1,)), ((), ()))
@@ -294,13 +296,13 @@
     ).astype(jnp.int32)
     outgoing = jnp.sum(slot_hits * within[:, None], axis=0).reshape(st_devices, slot_cap)
     incoming = lax.all_to_all(outgoing, "st", split_axis=0, concat_axis=0, tiled=True)
-    outgoing_rows = store_rows(
-        incoming.reshape(-1),
+    store = store_rows(
         document_corpus,
         document_rescale_factor,
         document_lookup_matrix,
         document_content_matrix,
     )
+    outgoing_rows = pick_rows(incoming.reshape(-1), store)
     (
         outgoing_rows,
         symbol_activations,

time: 151 us -> 149 us (0.987)
  waiting for transfers between devices: 58.4 us -> 53.1 us
  Pallas kernels: 21.5 us -> 23.1 us
    all_to_all x1, waiting for transfers between devices: 5.13 us -> 0.01 us  [local(): lax.all_to_all(outgoing, 'st', split_axis=0, concat_axis=0, tiled=True)]
    pallas_call x1 -> x2, Pallas kernels: 12.4 us -> 14.1 us  [the longest x1 10.1 us: store_rows(): pl.pallas_call(store_kernel, out_shape=jax.ShapeDtypeStruct((passage_coun...]
  transfers between devices with their start and end apart: 5 -> 5, of which waited for: 5 -> 4; matrix products, arithmetic and copies ran while one was open for 34% -> 35% of each run, Pallas kernels for 0% -> 7%
where the time goes in v3:
time: 149 us; the launch traced here: 148 us
  waiting for transfers between devices  53.1 us (36%)
  matrix products  29.5 us (20%)
  Pallas kernels  23.1 us (16%)
  starting transfers between devices  16.3 us (11%)
  local copies, waits for them, and re-layouts  14.5 us (10%)
  other arithmetic  11 us (7%)
    all_to_all x1, waiting for transfers between devices, local(): lax.all_to_all(outgoing_rows, 'st', split_axis=0, concat_axis=0, tiled=True)  28 us
    ppermute x3, waiting for transfers between devices, gather_features(): pieces.append(lax.ppermute(piece, 'tp', pairs))  25.1 us
    pallas_call x1, Pallas kernels, store_rows(): pl.pallas_call(store_kernel, out_shape=jax.ShapeDtypeStruct((passage_coun...  10.1 us
    pallas_call x1, Pallas kernels, attend(): pl.pallas_call(functools.partial(attend_kernel, reads), out_shape=jax.Sha...  9.06 us
    dot_general x6, matrix products, advance(): jnp.einsum('hsd,hse->hde', weighted_keys, value_part, precision=HIGHEST)  8.47 us
    dot_general x6, matrix products, advance(): jnp.einsum('hts,hse->hte', affinity_logits, value_part, precision=HIGHEST)  7.79 us
    all_to_all x1, starting transfers between devices, local(): lax.all_to_all(outgoing, 'st', split_axis=0, concat_axis=0, tiled=True)  7.28 us
    dot_general x1, matrix products, local(): projected = jnp.dot(token_piece, joined, preferred_element_type=jnp.float32)  6.18 us
  transfers between devices with their start and end apart: 5, of which 4 were waited for; matrix products, arithmetic and copies ran while one was open for 35% of the time, Pallas kernels for 7%

profile of v3, /device:TPU:0, one launch (start us, length us, event | category | flops | bytes accessed | tf_op | source)
XLA Modules:
  0.0 148.2 jit_solution(10285092104032171557)
XLA Ops:
  0.0 0.8 copy.64
  1.2 0.7 all_to_all.9
  1.9 7.3 %all-to-all-start = ((s32[8,1,6]{2,1,0:T(1,128)}), s32[8,1,6]{2,1,0:T(1,128)S(1)}, u32[]{:S(2)}, u32[]{:S(2)}) async-start(s32[8,1,6]{2,1,0:T(1,128)} %bitcast), calls=%async_computation | async-start | bytes 8192 | tf_op jit(solution)/shard_map/all_to_all | solution.py:298
  9.2 1.3 dynamic-slice_bitcast_fusion.5.refs_7_
  10.4 10.1 %shard_map.154.held = bf16[16,96,512]{2,1,0:T(8,128)(2,1)} custom-call(bf16[16,96,2048]{2,1,0:T(8,128)(2,1)} %rows_ref.1, f32[1,2048]{1,0:T(1,128)} %bitcast.165, bf16[2048,256]{1,0:T(8,128)(2,1)} %key_weight_ref.1, bf16[2048,256]{1,0:T(8,128)(2,1)} %value_weight_ref.1), custom_call_target="tpu_custom_call" | custom-call | flops 3221225472 | bytes 6291456 | tf_op jit(solution)/shard_map/pallas_call | solution.py:111
  20.5 0.5 broadcast.215
  21.1 0.7 reduce.10
  21.7 0.6 reshape.208.incoming
  22.3 4.0 %shard_map.155 = bf16[48,96,512]{2,1,0:T(8,128)(2,1)} custom-call(s32[48]{0:T(128)} %reshape.208.incoming, bf16[16,96,512]{2,1,0:T(8,128)(2,1)} %shard_map.154.held), custom_call_target="tpu_custom_call" | custom-call | tf_op jit(solution)/shard_map/pallas_call | solution.py:159
  26.4 1.6 %collective-permute-start.1 = (bf16[768,512]{1,0:T(8,128)(2,1)}, bf16[768,512]{1,0:T(8,128)(2,1)}, u32[]{:S(2)}, u32[]{:S(2)}) collective-permute-start(bf16[768,512]{1,0:T(8,128)(2,1)} %param.18), channel_id=1, source_target_pairs={{2,0},{3,1},{0,2},{1,3},{6,4},{7,5},{4,6},{5,7},{10,8},{11,9},{8,1... | collective-permute-start | bytes 2359304 | tf_op jit(solution)/shard_map/ppermute | solution.py:249
  28.0 1.4 collective-permute-start
  29.4 6.0 %all-to-all-start.1 = ((bf16[48,96,512]{2,1,0:T(8,128)(2,1)}), bf16[48,96,512]{2,1,0:T(8,128)(2,1)}, u32[]{:S(2)}, u32[]{:S(2)}) async-start(bf16[48,96,512]{2,1,0:T(8,128)(2,1)} %shard_map.155), calls=%async_computation.1 | async-start | bytes 9437184 | tf_op jit(solution)/shard_map/all_to_all | solution.py:371
  35.6 1.4 constant_dynamic-update-slice_fusion.2
  37.3 8.6 %collective-permute-done.2 = bf16[768,512]{1,0:T(8,128)(2,1)} collective-permute-done((bf16[768,512]{1,0:T(8,128)(2,1)}, bf16[768,512]{1,0:T(8,128)(2,1)}, u32[]{:S(2)}, u32[]{:S(2)}) %collective-permute-start.2) | collective-permute-done | bytes 786464 | tf_op jit(solution)/shard_map/ppermute | solution.py:249
  45.9 1.3 collective-permute-done.1
  47.2 15.2 %collective-permute-done = bf16[768,512]{1,0:T(8,128)(2,1)} collective-permute-done((bf16[768,512]{1,0:T(8,128)(2,1)}, bf16[768,512]{1,0:T(8,128)(2,1)}, u32[]{:S(2)}, u32[]{:S(2)}) %collective-permute-start) | collective-permute-done | bytes 786464 | tf_op jit(solution)/shard_map/ppermute | solution.py:249
  62.4 1.8 %pad_maximum_fusion = bf16[4,768,512]{2,1,0:T(8,128)(2,1)S(1)} fusion(bf16[1,768,512]{2,1,0:T(8,128)(2,1)} %bitcast.5, bf16[1,768,512]{2,1,0:T(8,128)(2,1)} %bitcast.4, bf16[1,768,512]{2,1,0:T(8,128)(2,1)} %bitcast.3, bf16[1,768,512]{2,1,0:T(8,128)(2,1)S(1)} %bitcast.154), kind=kLoop, calls=%fused_computation.48 | loop fusion | flops 4718592 | bytes 6291456 | tf_op jit(solution)/shard_map/stack | solution.py:250
  64.5 6.2 %fusion.41 = (bf16[768,1280]{1,0:T(8,128)(2,1)S(1)}, f32[768,1280]{1,0:T(8,128)}) fusion(bf16[2048,1280]{1,0:T(8,128)(2,1)S(1)} %constant_dynamic-update-slice_fusion, bf16[768,512]{1,0:T(8,128)(2,1)S(1)} %get-tuple-element.179, bf16[768,512]{1,0:T(8,128)(2,1)S(1)} %get-tuple-element.180, bf16[768,512]{1,0:T(8,128)(2,1)S(1)} %get-tuple-element.181, ...), kind=kOutput, calls=%fused_computation.94 | convolution fusion | flops 4040097792 | bytes 14286848 | tf_op jit(solution)/shard_map/dot_general | solution.py:336
  70.7 1.1 convert_bitcast_fusion
  71.9 0.9 convolution_add_fusion.2
  72.8 0.8 dynamic-slice_bitcast_fusion.4
  73.6 2.1 %copy_bitcast_fusion.1 = (f32[768,2,128]{2,0,1:T(8,128)S(1)}, f32[768,2,128]{2,0,1:T(8,128)}) fusion(f32[96,2,8,128]{3,2,1,0:T(8,128)S(1)} %get-tuple-element.182, f32[96,2,8,128]{3,2,1,0:T(8,128)} %get-tuple-element.183), kind=kLoop, calls=%fused_computation.52 | loop fusion | bytes 3145728 | tf_op jit(solution)/shard_map/transpose | solution.py:30
  75.7 31.9 %while.17 = (s32[]{:T(128)}, f32[2,128,128]{2,1,0:T(8,128)S(1)}, f32[2,128]{1,0:T(2,128)S(1)}, f32[2]{0:T(128)S(1)}, f32[6,2,128,128]{3,2,0,1:T(8,128)S(1)}, /*i...) while((s32[]{:T(128)}, f32[2,128,128]{2,1,0:T(8,128)S(1)}, ...), condition=%wide.region_7.8_spmd.clone, body=%wide.region_2.7_spmd.clone.sunk | while | flops 202557696 | bytes 2339037 | solution.py:72
  76.3 0.4 fusion.67
  76.7 0.3 fusion.68
  77.9 1.4 convolution_add_fusion.4
  79.7 1.3 fusion.70
  81.6 0.4 fusion.67
  82.0 0.3 fusion.68
  83.2 1.4 convolution_add_fusion.4
  85.0 1.3 fusion.70
  86.9 0.4 fusion.67
  87.3 0.3 fusion.68
  88.6 1.4 convolution_add_fusion.4
  90.3 1.3 fusion.70
  92.2 0.4 fusion.67
  93.9 1.4 convolution_add_fusion.4
  95.7 1.3 fusion.70
  97.5 0.4 fusion.67
  99.2 1.4 convolution_add_fusion.4
  101.0 1.3 fusion.70
  102.9 0.4 fusion.67
  104.5 1.4 convolution_add_fusion.4
  106.3 1.3 fusion.70
  107.6 2.1 %slice.38.refs_5_ = f32[768,256]{1,0:T(8,128)} slice(f32[768,1280]{1,0:T(8,128)} %get-tuple-element.190), slice={[0:768], [1024:1280]} | slice | bytes 1572864 | tf_op jit(solution)/shard_map/slice | solution.py:342
  110.3 0.9 copy_bitcast_fusion.refs_6_
  111.2 28.0 %all-to-all-done.1.refs_0_.refs_1_.refs_2_.refs_3_ = bf16[48,96,512]{2,1,0:T(8,128)(2,1)} async-done(((bf16[48,96,512]{2,1,0:T(8,128)(2,1)}), bf16[48,96,512]{2,1,0:T(8,128)(2,1)}, u32[]{:S(2)}, u32[]{:S(2)}) %all-to-all-start.1) | async-done | bytes 4718624 | tf_op jit(solution)/shard_map/all_to_all | solution.py:371
  139.2 9.1 %shard_map.156 = bf16[768,256]{1,0:T(8,128)(2,1)} custom-call(s32[24]{0:T(128)} %copy-done.7, bf16[48,96,512]{2,1,0:T(8,128)(2,1)} %all-to-all-done.1.refs_0_.refs_1_.refs_2_.refs_3_, bf16[48,96,512]{2,1,0:T(8,128)(2,1)} %all-to-all-done.1.refs_0_.refs_1_.refs_2_.refs_3_, bf16[48,96,512]{2,1,0:T(8,128)(2,1)} %all-to-all-done.1.refs_0_.refs_1_.refs_2_.refs_3_, ...), custom_call_target="tpu_custom_call" | custom-call | flops 301989888 | bytes 9437184 | tf_op jit(solution)/shard_map/pallas_call | solution.py:217
  (128 shorter events, 13.4 us)
Async XLA Ops:
  0.0 71.9 %copy-start = (bf16[2048,16]{0,1:T(8,128)(2,1)S(1)}, bf16[2048,16]{0,1:T(8,128)(2,1)}, u32[]{:S(2)}) copy-start(bf16[2048,16]{0,1:T(8,128)(2,1)} %param.24) | copy-start | bytes 196612
  1.1 19.5 %copy-start.7 = (s32[24]{0:T(128)}, s32[24]{0:T(128)S(1)}, u32[]{:S(2)}) copy-start(s32[24]{0:T(128)S(1)} %multiply_add_fusion.1.slot_ref) | copy-start | bytes 292
  1.9 18.7 %all-to-all-start = ((s32[8,1,6]{2,1,0:T(1,128)}), s32[8,1,6]{2,1,0:T(1,128)S(1)}, u32[]{:S(2)}, u32[]{:S(2)}) async-start(s32[8,1,6]{2,1,0:T(1,128)} %bitcast), calls=%async_computation | async-start | bytes 8192 | tf_op jit(solution)/shard_map/all_to_all | solution.py:298
  26.3 9.0 %copy-start.1 = (bf16[2048,256]{1,0:T(8,128)(2,1)S(1)}, bf16[2048,256]{1,0:T(8,128)(2,1)}, u32[]{:S(2)}) copy-start(bf16[2048,256]{1,0:T(8,128)(2,1)} %param.21) | copy-start | bytes 3145732
  26.3 9.2 %copy-start.2 = (bf16[2048,256]{1,0:T(8,128)(2,1)S(1)}, bf16[2048,256]{1,0:T(8,128)(2,1)}, u32[]{:S(2)}) copy-start(bf16[2048,256]{1,0:T(8,128)(2,1)} %param.22) | copy-start | bytes 3145732
  26.3 19.6 %collective-permute-start.2 = (bf16[768,512]{1,0:T(8,128)(2,1)}, bf16[768,512]{1,0:T(8,128)(2,1)}, u32[]{:S(2)}, u32[]{:S(2)}) collective-permute-start(bf16[768,512]{1,0:T(8,128)(2,1)} %param.18), channel_id=1, source_target_pairs={{3,0},{0,1},{1,2},{2,3},{7,4},{4,5},{5,6},{6,7},{11,8},{8,9},{9,10... | collective-permute-start | bytes 2359304 | tf_op jit(solution)/shard_map/ppermute | solution.py:249
  26.4 20.8 %collective-permute-start.1 = (bf16[768,512]{1,0:T(8,128)(2,1)}, bf16[768,512]{1,0:T(8,128)(2,1)}, u32[]{:S(2)}, u32[]{:S(2)}) collective-permute-start(bf16[768,512]{1,0:T(8,128)(2,1)} %param.18), channel_id=1, source_target_pairs={{2,0},{3,1},{0,2},{1,3},{6,4},{7,5},{4,6},{5,7},{10,8},{11,9},{8,1... | collective-permute-start | bytes 2359304 | tf_op jit(solution)/shard_map/ppermute | solution.py:249
  28.0 34.4 %collective-permute-start = (bf16[768,512]{1,0:T(8,128)(2,1)}, bf16[768,512]{1,0:T(8,128)(2,1)}, u32[]{:S(2)}, u32[]{:S(2)}) collective-permute-start(bf16[768,512]{1,0:T(8,128)(2,1)} %param.18), channel_id=1, source_target_pairs={{1,0},{2,1},{3,2},{0,3},{5,4},{6,5},{7,6},{4,7},{9,8},{10,9},{11,1... | collective-permute-start | bytes 2359304 | tf_op jit(solution)/shard_map/ppermute | solution.py:249
  29.4 109.8 %all-to-all-start.1 = ((bf16[48,96,512]{2,1,0:T(8,128)(2,1)}), bf16[48,96,512]{2,1,0:T(8,128)(2,1)}, u32[]{:S(2)}, u32[]{:S(2)}) async-start(bf16[48,96,512]{2,1,0:T(8,128)(2,1)} %shard_map.155), calls=%async_computation.1 | async-start | bytes 9437184 | tf_op jit(solution)/shard_map/all_to_all | solution.py:371
  35.4 1.7 %copy-start.3 = (bf16[2048,256]{1,0:T(8,128)(2,1)S(1)}, bf16[2048,256]{1,0:T(8,128)(2,1)}, u32[]{:S(2)}) copy-start(bf16[2048,256]{1,0:T(8,128)(2,1)} %param.28) | copy-start | bytes 3145732
  35.4 1.8 %copy-start.4 = (bf16[2048,256]{1,0:T(8,128)(2,1)S(1)}, bf16[2048,256]{1,0:T(8,128)(2,1)}, u32[]{:S(2)}) copy-start(bf16[2048,256]{1,0:T(8,128)(2,1)} %param.33) | copy-start | bytes 3145732
  35.4 27.1 %copy-start.5 = (bf16[768,512]{1,0:T(8,128)(2,1)S(1)}, bf16[768,512]{1,0:T(8,128)(2,1)}, u32[]{:S(2)}) copy-start(bf16[768,512]{1,0:T(8,128)(2,1)} %param.18) | copy-start | bytes 2359300
  64.5 7.4 %copy-start.8 = (f32[16]{0:T(128)S(1)}, f32[16]{0:T(128)}, u32[]{:S(2)}) copy-start(f32[16]{0:T(128)} %param.25) | copy-start | bytes 196
  75.7 34.2 %copy-start.6 = (f32[256]{0:T(256)S(1)}, f32[256]{0:T(256)}, u32[]{:S(2)}) copy-start(f32[256]{0:T(256)} %param.27) | copy-start | bytes 3076
